TPU v7x, 256 devices: a 4x2x16 block of a 4x16x16 slice. The times are simulated.
256 devices in a mesh: grp: 2 (over y), ep: 64 (over z, x), tp: 2 (over core).
Axes of the slice: x: 4, y: 2, z: 16, core: 2. Of those that a mesh axis runs over, the one named last changes fastest.
The devices are a block of a 4x16x16 slice.
Arguments:
- tokens: bfloat16 [2048, 1024], P(('grp', 'ep')), parts along dimension 0, may hold values from -6 to 6
- query_weight: bfloat16 [1024, 512], P(None, 'tp'), may hold values from -0.1875 to 0.1875
- key_weight: bfloat16 [1024, 512], P(None, 'tp'), may hold values from -0.1875 to 0.1875
- value_weight: bfloat16 [1024, 512], P(None, 'tp'), may hold values from -0.1875 to 0.1875
- outgate_weight: bfloat16 [1024, 512], P(None, 'tp'), may hold values from -0.1875 to 0.1875
- ingate_weight: bfloat16 [1024, 4], P(None, 'tp'), may hold values from -0.1875 to 0.1875
- forget_weight: bfloat16 [1024, 4], P(None, 'tp'), may hold values from -0.1875 to 0.1875
- forget_bias: float32 [4], P('tp'), may hold values from -2 to 5
- head_gain: float32 [4, 128], P('tp'), may hold values from 0.1 to 1.9
- merge_weight: bfloat16 [512, 1024], P('tp'), may hold values from -0.25 to 0.25
- mixer_gain: float32 [1024], replicated, may hold values from 0.1 to 1.9
- feed_gain: float32 [1024], replicated, may hold values from 0.1 to 1.9
- memory_matrix: float32 [2048, 4, 128, 128], P(('grp', 'ep'), 'tp'), parts along dimension 0, may hold values from -0.6 to 0.6
- memory_norm: float32 [2048, 4, 128], P(('grp', 'ep'), 'tp'), parts along dimension 0, may hold values from -0.6 to 0.6
- memory_max: float32 [2048, 4], P(('grp', 'ep'), 'tp'), parts along dimension 0, may hold values from -4 to 4
- routes: int32 [2048, 2], P(('grp', 'ep')), parts along dimension 0, may hold values from 0 to 63, all different within a row; in each aligned block of 16 rows (0 to 15, 16 to 31, ...) at most 2 rows name the same one
- route_scores: bfloat16 [2048, 2], P(('grp', 'ep')), parts along dimension 0, may hold values from -4 to 4
- expert_gate: bfloat16 [64, 1024, 1792], P('ep', None, 'tp'), may hold values from -0.1875 to 0.1875
- expert_up: bfloat16 [64, 1024, 1792], P('ep', None, 'tp'), may hold values from -0.1875 to 0.1875
- expert_down: bfloat16 [64, 1792, 1024], P('ep', 'tp'), may hold values from -0.125 to 0.125
- dense_left: bfloat16 [1024, 2816], P(None, 'ep'), may hold values from -0.1875 to 0.1875
- dense_right: bfloat16 [1024, 2816], P(None, 'ep'), may hold values from -0.1875 to 0.1875
- dense_down: bfloat16 [2816, 1024], P('ep'), may hold values from -0.109375 to 0.109375
- blend_weight: float32 [1024], replicated, may hold values from -0.1875 to 0.1875
Outputs:
- layer_out: bfloat16 [2048, 1024], P(('grp', 'ep', 'tp')), parts along dimension 0
- new_matrix: float32 [2048, 4, 128, 128], P(('grp', 'ep'), 'tp'), parts along dimension 0
- new_norm: float32 [2048, 4, 128], P(('grp', 'ep'), 'tp'), parts along dimension 0
- new_max: float32 [2048, 4], P(('grp', 'ep'), 'tp'), parts along dimension 0
There are 2 independent parts, one for each index of `grp`. A program takes and returns all parts, laid end to end along the dimension named above; an argument that names none is the same for every part. Nothing has to cross between parts.
Inputs may be any that keep to these rules, and one draw needn't show every extreme that they name: `routes`: each row names 2 different experts. Among the rows of one device (aligned blocks of 16 rows) no expert is named more than 2 times, and in every draw some expert is named exactly 2 times in some block.
All inputs are finite; a program needn't handle non-finite values.
Results may differ from a plain program's by a relative error of at most 0.014.
Values may be sent and summed in bfloat16 or wider, within the bound.
A program may use at most 64 MiB of HBM per device.

v0:
```python
import jax
import jax.numpy as jnp
from jax import lax
from jax.sharding import Mesh
from jax.sharding import PartitionSpec as P

EP = ("ep_0", "ep_1")
GRP_EP = ("grp", "ep_0", "ep_1")
GRP_EP_TP = ("grp", "ep_0", "ep_1", "tp")


epsilon = 1e-06


def copy_for_each(shard, axis):
    copies = jnp.broadcast_to(shard, (lax.axis_size(axis), *shard.shape))
    return lax.all_to_all(copies, axis, split_axis=0, concat_axis=0, tiled=True)


def over_copies(shard, axis):
    everything = copy_for_each(shard, axis)
    return jnp.sum(everything.astype(jnp.float32), axis=0)


def whole_of(shard, axes, dim):
    for axis in reversed(axes):
        shard = lax.all_gather(shard, axis, axis=dim, tiled=True)
    return shard


def split_up(shard, dim, length):
    before, after = (shard.shape[:dim], shard.shape[dim + 1 :])
    return jnp.moveaxis(shard.reshape(*before, length, -1, *after), dim, 0)


def sent_and_summed(shard, axis, dim):
    tiles = split_up(shard, dim, lax.axis_size(axis))
    arrived = lax.all_to_all(tiles, axis, split_axis=0, concat_axis=0, tiled=True)
    return arrived.astype(jnp.float32).sum(axis=0)


def rms_norm(values, gains):
    floats = values.astype(jnp.float32)
    scaled = floats * lax.rsqrt(jnp.mean(floats * floats, axis=-1, keepdims=True) + epsilon)
    return (scaled * gains).astype(jnp.bfloat16)


def memory_step(query_rows, key_rows, value_rows, in_gate, forget_pre, matrix, norm_vec, old_max):
    log_forget = jax.nn.log_sigmoid(forget_pre)
    new_max = jnp.maximum(log_forget + old_max, in_gate)
    keep = jnp.exp(log_forget + old_max - new_max)
    write = jnp.exp(in_gate - new_max)
    matrix = (
        keep[..., None, None] * matrix
        + write[..., None, None] * key_rows[..., :, None] * value_rows[..., None, :]
    )
    norm_vec = keep[..., None] * norm_vec + write[..., None] * key_rows
    numer = jnp.einsum("bhd,bhde->bhe", query_rows, matrix, precision=lax.Precision.HIGHEST)
    denom = jnp.sum(query_rows * norm_vec, axis=-1)
    readout = numer / jnp.maximum(jnp.abs(denom), jnp.exp(-new_max))[..., None]
    return (readout, matrix, norm_vec, new_max)


def dense_block(rows, dense_left, dense_right, dense_down):
    left_val = jnp.dot(rows, dense_left, preferred_element_type=jnp.float32)
    right_val = jnp.dot(rows, dense_right, preferred_element_type=jnp.float32)
    dense_hidden = (jax.nn.silu(left_val) * right_val).astype(jnp.bfloat16)
    return jnp.dot(dense_hidden, dense_down, preferred_element_type=jnp.float32)


def local(
    tokens,
    query_weight,
    key_weight,
    value_weight,
    outgate_weight,
    ingate_weight,
    forget_weight,
    forget_bias,
    head_gain,
    merge_weight,
    mixer_gain,
    feed_gain,
    memory_matrix,
    memory_norm,
    memory_max,
    routes,
    route_scores,
    expert_gate,
    expert_up,
    expert_down,
    dense_left,
    dense_right,
    dense_down,
    blend_weight,
):
    own_rows = tokens.shape[0]
    heads_here = forget_bias.shape[0]
    head_size = head_gain.shape[1]
    width_here = heads_here * head_size
    model_width = tokens.shape[1]
    normed = rms_norm(tokens, mixer_gain)

    def project(weight):
        return jnp.dot(normed, weight, preferred_element_type=jnp.float32)

    query = project(query_weight).reshape(own_rows, heads_here, head_size)
    key_rows = project(key_weight).reshape(own_rows, heads_here, head_size) * head_size ** (-0.5)
    value_rows = project(value_weight).reshape(own_rows, heads_here, head_size)
    outgate_rows = project(outgate_weight).reshape(own_rows, heads_here, head_size)
    in_gate = project(ingate_weight)
    forget_pre = project(forget_weight) + forget_bias
    readout, matrix, norm_vec, new_max = memory_step(
        query, key_rows, value_rows, in_gate, forget_pre, memory_matrix, memory_norm, memory_max
    )
    energy = jnp.sum(readout * readout, axis=(1, 2))
    gated = (
        (readout * head_gain * jax.nn.sigmoid(outgate_rows))
        .reshape(own_rows, width_here)
        .astype(jnp.bfloat16)
    )
    head_part = jnp.dot(gated, merge_weight, preferred_element_type=jnp.float32)
    head_total, energy_total = (
        over_copies(head_part.astype(jnp.bfloat16), "tp").astype(jnp.float32),
        over_copies(energy.astype(jnp.bfloat16), "tp").astype(jnp.float32),
    )
    all_width = width_here * lax.axis_size("tp")
    head_scale = lax.rsqrt(energy_total / all_width + epsilon)
    resid = (tokens.astype(jnp.float32) + head_scale[:, None] * head_total).astype(jnp.bfloat16)
    normed2 = rms_norm(resid, feed_gain)
    pick_count = routes.shape[1]
    expert_count = lax.axis_size(EP)
    slot_count = max(2, 3 * own_rows * pick_count // (2 * expert_count))
    half_rows = own_rows // lax.axis_size("tp")
    first_row = lax.axis_index("tp") * half_rows
    flat_routes = routes.reshape(own_rows * pick_count)
    member = (flat_routes[:, None] == jnp.arange(expert_count, dtype=jnp.int32)[None, :]).astype(
        jnp.int32
    )
    slot_rank = jnp.sum(member * (jnp.cumsum(member, axis=0) - member), axis=1)
    target = flat_routes * slot_count + slot_rank
    chooser = (
        target[:, None] == jnp.arange(expert_count * slot_count, dtype=jnp.int32)[None, :]
    ).astype(jnp.bfloat16)
    spread_rows = jnp.repeat(normed2, pick_count, axis=0)
    outbox = jnp.einsum("as,ad->sd", chooser, spread_rows, preferred_element_type=jnp.float32)
    outbox = outbox.astype(jnp.bfloat16).reshape(expert_count, slot_count, model_width)
    inbox = lax.all_to_all(outbox, EP, split_axis=0, concat_axis=0, tiled=True)
    sources, slots, width = inbox.shape
    rows = inbox.reshape(sources * slots, width)
    gate_val = jnp.dot(rows, expert_gate[0], preferred_element_type=jnp.float32)
    up_val = jnp.dot(rows, expert_up[0], preferred_element_type=jnp.float32)
    hidden = (jax.nn.silu(gate_val) * up_val).astype(jnp.bfloat16)
    expert_part = jnp.dot(hidden, expert_down[0], preferred_element_type=jnp.float32)
    expert_total = over_copies(expert_part.astype(jnp.bfloat16), "tp").astype(jnp.float32)
    results = expert_total.astype(jnp.bfloat16).reshape(sources, slots, width)
    returned = lax.all_to_all(results, EP, split_axis=0, concat_axis=0, tiled=True)
    picked = jnp.dot(
        chooser,
        returned.reshape(expert_count * slot_count, model_width),
        preferred_element_type=jnp.float32,
    )
    route_weight = jax.nn.softmax(route_scores.astype(jnp.float32), axis=-1)
    routed = jnp.sum(
        route_weight[..., None] * picked.reshape(own_rows, pick_count, model_width), axis=1
    )
    own_half = lax.dynamic_slice_in_dim(normed2, first_row, half_rows, 0)
    terms = dense_block(whole_of(own_half, EP, 0), dense_left, dense_right, dense_down)
    after_scale = jax.nn.sigmoid(jnp.sum(own_half.astype(jnp.float32) * blend_weight, axis=-1))[
        :, None
    ]
    after_add = lax.dynamic_slice_in_dim(routed, first_row, half_rows, 0)
    summed = sent_and_summed(terms.astype(jnp.bfloat16), EP, 0)
    resid_half = lax.dynamic_slice_in_dim(resid, first_row, half_rows, 0).astype(jnp.float32)
    layer_out = (resid_half + after_add + after_scale * summed).astype(jnp.bfloat16)
    return (layer_out, matrix, norm_vec, new_max)


def solution(mesh):
    split = Mesh(
        mesh.devices.reshape(mesh.shape["grp"], 16, 4, mesh.shape["tp"]),
        ("grp", "ep_0", "ep_1", "tp"),
    )
    return jax.shard_map(
        local,
        mesh=split,
        in_specs=(
            P(GRP_EP, None),
            P(None, "tp"),
            P(None, "tp"),
            P(None, "tp"),
            P(None, "tp"),
            P(None, "tp"),
            P(None, "tp"),
            P("tp"),
            P("tp", None),
            P("tp", None),
            P(),
            P(),
            P(GRP_EP, "tp", None, None),
            P(GRP_EP, "tp", None),
            P(GRP_EP, "tp"),
            P(GRP_EP, None),
            P(GRP_EP, None),
            P(EP, None, "tp"),
            P(EP, None, "tp"),
            P(EP, "tp", None),
            P(None, EP),
            P(None, EP),
            P(EP, None),
            P(),
        ),
        out_specs=(
            P(GRP_EP_TP, None),
            P(GRP_EP, "tp", None, None),
            P(GRP_EP, "tp", None),
            P(GRP_EP, "tp"),
        ),
        check_vma=False,
    )
```

profile of v0, /device:TPU:40, one launch (start us, length us, event | category | flops | bytes accessed | tf_op | source)
XLA Modules:
  0.0 217.8 jit_solution(13244536112566554732)
XLA Ops:
  7.2 0.0 copy-start
  7.2 1.0 fusion.38
  8.2 1.3 fusion.64
  9.6 1.3 fusion.57
  10.9 1.0 fusion.61
  11.9 1.0 subtract_exponential_fusion.1
  12.9 0.0 copy-start.13
  12.9 0.1 copy.72
  13.0 1.3 fusion.59
  14.3 0.1 copy.73
  14.4 0.7 multiply_reduce_fusion.2
  15.1 0.1 copy.75
  15.2 0.1 copy.76
  15.3 2.0 multiply_add_fusion
  17.3 0.0 copy-start.1
  17.3 0.0 copy-start.2
  17.3 0.0 copy-start.8
  17.3 0.0 copy-start.14
  17.3 1.2 copy-done.1
  18.6 1.9 fusion.67
  20.5 0.3 multiply_reduce_fusion.1
  20.8 0.6 broadcast_in_dim.8
  21.3 3.2 %all-to-all-start = ((bf16[2,1,16]{2,1,0:T(2,128)(2,1)}), bf16[2,1,16]{2,1,0:T(2,128)(2,1)S(1)}, u32[]{:S(2)}, u32[]{:S(2)}) async-start(bf16[2,1,16]{2,1,0:T(2,128)(2,1)} %broadcast_in_dim.8), calls=%async_computation | async-start | bytes 2048 | tf_op jit(solution)/shard_map/all_to_all | solution.py:17
  24.6 0.2 fusion.22
  24.9 0.2 convolution_convert_fusion.2
  25.1 0.8 all-to-all-done
  25.8 0.6 broadcast_in_dim.9
  26.5 3.3 %all-to-all-start.1 = ((bf16[2,16,1024]{2,1,0:T(8,128)(2,1)}), bf16[2,16,1024]{2,1,0:T(8,128)(2,1)S(1)}, u32[]{:S(2)}, u32[]{:S(2)}) async-start(bf16[2,16,1024]{2,1,0:T(8,128)(2,1)} %broadcast_in_dim.9), calls=%async_computation.1 | async-start | bytes 131072 | tf_op jit(solution)/shard_map/all_to_all | solution.py:17
  29.8 1.4 all-to-all-done.1
  31.2 0.2 fusion.35
  31.4 0.1 fusion.37
  31.6 0.1 copy.78
  31.6 0.1 eq.50
  31.7 0.1 fusion.43
  31.8 0.1 reduce_window_sum.11
  31.9 0.2 select_reduce_fusion
  32.1 0.3 convolution_convert_fusion.1
  32.4 0.8 reshape.135
  33.2 29.0 %all-to-all-start.2 = ((bf16[64,2,1024]{2,1,0:T(2,128)(2,1)}), bf16[64,2,1024]{2,1,0:T(2,128)(2,1)S(1)}, u32[]{:S(2)}, u32[]{:S(2)}) async-start(bf16[64,2,1024]{2,1,0:T(2,128)(2,1)} %reshape.135), calls=%async_computation.2 | async-start | bytes 524288 | tf_op jit(solution)/shard_map/all_to_all | solution.py:148
  62.3 0.1 all-gather.2.cloned.1.call-start
  62.4 0.1 multiply_reduce_fusion
  62.5 12.7 %all_gather.6 = bf16[32,1024]{1,0:T(8,128)(2,1)} all-gather(bf16[8,1024]{1,0:T(8,128)(2,1)S(1)} %get-tuple-element.5), channel_id=1, replica_groups=mesh['grp'=2,'ep_0'=16,'ep_1'=4,'tp'=2] {'ep_1'}, dimensions={0}, use_global_device_ids=true | all-gather | bytes 81920 | tf_op jit(solution)/shard_map/all_gather | solution.py:27
  75.2 0.1 all-gather.2.cloned.1.call-update
  75.2 8.5 %all-to-all-done.2 = bf16[64,2,1024]{2,1,0:T(2,128)(2,1)S(1)} async-done(((bf16[64,2,1024]{2,1,0:T(2,128)(2,1)}), bf16[64,2,1024]{2,1,0:T(2,128)(2,1)S(1)}, u32[]{:S(2)}, u32[]{:S(2)}) %all-to-all-start.2) | async-done | bytes 262176 | tf_op jit(solution)/shard_map/all_to_all | solution.py:148
  83.8 0.1 reshape.136
  83.9 2.0 fusion.4
  85.8 2.3 %fusion.10 = bf16[128,1024]{1,0:T(8,128)(2,1)S(1)} fusion(bf16[1,896,1024]{2,1,0:T(8,128)(2,1)S(1)} %copy-done, bf16[128,1024]{1,0:T(8,128)(2,1)S(1)} %reshape.136, bf16[1,1024,896]{2,1,0:T(8,128)(2,1)} %param.42, f32[128,896]{1,0:T(8,128)S(1)} %fusion.4), kind=kOutput, calls=%fused_computation.11 | convolution fusion | flops 470581248 | bytes 4653056 | tf_op jit(solution)/shard_map/dot_general | solution.py:154
  88.2 0.1 broadcast_in_dim.11
  88.2 0.0 copy-start.6
  88.2 4.3 %all_to_all.31 = bf16[2,128,1024]{2,1,0:T(8,128)(2,1)S(1)} all-to-all(bf16[2,128,1024]{2,1,0:T(8,128)(2,1)S(1)} %broadcast_in_dim.11), channel_id=1, replica_groups=mesh['grp'=2,'ep_0'=16,'ep_1'=4,'tp'=2] {'tp'}, dimensions={0} | all-to-all | bytes 1048576 | tf_op jit(solution)/shard_map/all_to_all | solution.py:17
  92.5 0.1 reduce_sum.122
  92.6 0.8 reshape.137
  93.5 7.3 %all-to-all-start.4 = ((bf16[64,2,1024]{2,1,0:T(2,128)(2,1)}), bf16[64,2,1024]{2,1,0:T(2,128)(2,1)S(1)}, u32[]{:S(2)}, u32[]{:S(2)}) async-start(bf16[64,2,1024]{2,1,0:T(2,128)(2,1)} %reshape.137), calls=%async_computation.4 | async-start | bytes 524288 | tf_op jit(solution)/shard_map/all_to_all | solution.py:157
  100.8 47.5 %all-gather.2.cloned.1.call-done = bf16[512,1024]{1,0:T(8,128)(2,1)} async-done(((bf16[32,1024]{1,0:T(8,128)(2,1)}), bf16[512,1024]{1,0:T(8,128)(2,1)}) %all-gather.2.cloned.1.call-update) | async-done | bytes 1048592 | tf_op jit(solution)/shard_map/all_gather | solution.py:27
  148.3 1.7 fusion.68
  150.0 3.2 %fusion.6 = bf16[64,8,1024]{2,1,0:T(8,128)(2,1)} fusion(bf16[44,1024]{1,0:T(8,128)(2,1)S(1)} %copy-done.5, bf16[512,1024]{1,0:T(8,128)(2,1)} %all-gather.2.cloned.1.call-done, bf16[1024,44]{0,1:T(8,128)(2,1)S(1)} %copy-done.6, f32[512,44]{0,1:T(8,128)S(1)} %fusion.68), kind=kOutput, calls=%fused_computation.9 | convolution fusion | flops 92934144 | bytes 2367488 | tf_op jit(solution)/shard_map/dot_general | solution.py:68
  153.2 11.6 %all-to-all-start.5 = ((bf16[64,8,1024]{2,1,0:T(8,128)(2,1)}), bf16[64,8,1024]{2,1,0:T(8,128)(2,1)S(1)}, u32[]{:S(2)}, u32[]{:S(2)}) async-start(bf16[64,8,1024]{2,1,0:T(8,128)(2,1)} %fusion.6), calls=%async_computation.5 | async-start | bytes 2097152 | tf_op jit(solution)/shard_map/all_to_all | solution.py:38
  164.8 0.1 reduce_sum.120
  164.9 0.1 copy.79
  165.0 0.1 reshape.142
  165.1 0.2 fusion.18
  165.3 44.8 %all-to-all-done.5 = bf16[64,8,1024]{2,1,0:T(8,128)(2,1)S(1)} async-done(((bf16[64,8,1024]{2,1,0:T(8,128)(2,1)}), bf16[64,8,1024]{2,1,0:T(8,128)(2,1)S(1)}, u32[]{:S(2)}, u32[]{:S(2)}) %all-to-all-start.5) | async-done | bytes 1048608 | tf_op jit(solution)/shard_map/all_to_all | solution.py:38
  210.1 0.2 convert_reduce_fusion
  210.3 0.7 add_convert_fusion
  (47 shorter events, 0.4 us)
Async XLA Ops:
  7.2 78.7 %copy-start = (bf16[1,896,1024]{2,1,0:T(8,128)(2,1)S(1)}, bf16[1,896,1024]{2,1,0:T(8,128)(2,1)}, u32[]{:S(2)}) copy-start(bf16[1,896,1024]{2,1,0:T(8,128)(2,1)} %param.43) | copy-start | bytes 5505028
  7.2 7.2 %copy-start.9 = (f32[16,2,128]{2,1,0:T(2,128)S(1)}, f32[16,2,128]{2,1,0:T(2,128)}, u32[]{:S(2)}) copy-start(f32[16,2,128]{2,1,0:T(2,128)} %param.37) | copy-start | bytes 49156
  12.9 4.4 %copy-start.13 = (f32[16,2]{0,1:T(2,128)}, f32[16,2]{0,1:T(2,128)S(1)}, u32[]{:S(2)}) copy-start(f32[16,2]{0,1:T(2,128)S(1)} %get-tuple-element.14) | copy-start | bytes 388
  17.3 1.3 copy-start.1
  17.3 7.3 %copy-start.2 = (bf16[16,1024]{1,0:T(8,128)(2,1)S(1)}, bf16[16,1024]{1,0:T(8,128)(2,1)}, u32[]{:S(2)}) copy-start(bf16[16,1024]{1,0:T(8,128)(2,1)} %param.24) | copy-start | bytes 98308
  17.3 7.3 %copy-start.3 = (bf16[1024,256]{1,0:T(8,128)(2,1)S(1)}, bf16[1024,256]{1,0:T(8,128)(2,1)}, u32[]{:S(2)}) copy-start(bf16[1024,256]{1,0:T(8,128)(2,1)} %param.28) | copy-start | bytes 1572868
  17.3 7.3 %copy-start.8 = (f32[1024]{0:T(1024)S(1)}, f32[1024]{0:T(1024)}, u32[]{:S(2)}) copy-start(f32[1024]{0:T(1024)} %param.34) | copy-start | bytes 12292
  17.3 7.6 %copy-start.14 = (f32[2,128]{1,0:T(2,128)S(1)}, f32[2,128]{1,0:T(2,128)}, u32[]{:S(2)}) copy-start(f32[2,128]{1,0:T(2,128)} %param.32) | copy-start | bytes 3076
  17.3 7.6 %copy-start.4 = (bf16[256,1024]{1,0:T(8,128)(2,1)S(1)}, bf16[256,1024]{1,0:T(8,128)(2,1)}, u32[]{:S(2)}) copy-start(bf16[256,1024]{1,0:T(8,128)(2,1)} %param.33) | copy-start | bytes 1572868
  17.3 14.1 %copy-start.10 = (f32[1024]{0:T(1024)S(1)}, f32[1024]{0:T(1024)}, u32[]{:S(2)}) copy-start(f32[1024]{0:T(1024)} %param.35) | copy-start | bytes 12292
  18.6 13.0 %copy-start.12 = (s32[16,2]{0,1:T(2,128)S(1)}, s32[16,2]{0,1:T(2,128)}, u32[]{:S(2)}) copy-start(s32[16,2]{0,1:T(2,128)} %param.39) | copy-start | bytes 388
  20.5 41.9 %copy-start.11 = (f32[1024]{0:T(1024)S(1)}, f32[1024]{0:T(1024)}, u32[]{:S(2)}) copy-start(f32[1024]{0:T(1024)} %param.47) | copy-start | bytes 12292
  21.3 4.5 %all-to-all-start = ((bf16[2,1,16]{2,1,0:T(2,128)(2,1)}), bf16[2,1,16]{2,1,0:T(2,128)(2,1)S(1)}, u32[]{:S(2)}, u32[]{:S(2)}) async-start(bf16[2,1,16]{2,1,0:T(2,128)(2,1)} %broadcast_in_dim.8), calls=%async_computation | async-start | bytes 2048 | tf_op jit(solution)/shard_map/all_to_all | solution.py:17
  26.5 4.7 %all-to-all-start.1 = ((bf16[2,16,1024]{2,1,0:T(8,128)(2,1)}), bf16[2,16,1024]{2,1,0:T(8,128)(2,1)S(1)}, u32[]{:S(2)}, u32[]{:S(2)}) async-start(bf16[2,16,1024]{2,1,0:T(8,128)(2,1)} %broadcast_in_dim.9), calls=%async_computation.1 | async-start | bytes 131072 | tf_op jit(solution)/shard_map/all_to_all | solution.py:17
  33.2 50.5 %all-to-all-start.2 = ((bf16[64,2,1024]{2,1,0:T(2,128)(2,1)}), bf16[64,2,1024]{2,1,0:T(2,128)(2,1)S(1)}, u32[]{:S(2)}, u32[]{:S(2)}) async-start(bf16[64,2,1024]{2,1,0:T(2,128)(2,1)} %reshape.135), calls=%async_computation.2 | async-start | bytes 524288 | tf_op jit(solution)/shard_map/all_to_all | solution.py:148
  62.3 86.0 %all-gather.2.cloned.1.call-start = ((), (), s32[]{:S(2)}) async-start(), calls=%async_computation.6 | async-start | bytes 1114112 | tf_op jit(solution)/shard_map/all_gather | solution.py:27
  88.1 60.2 %copy-start.7 = (bf16[1024,44]{0,1:T(8,128)(2,1)S(1)}, bf16[1024,44]{0,1:T(8,128)(2,1)}, u32[]{:S(2)}) copy-start(bf16[1024,44]{0,1:T(8,128)(2,1)} %param.44) | copy-start | bytes 270340
  88.2 61.8 %copy-start.5 = (bf16[44,1024]{1,0:T(8,128)(2,1)S(1)}, bf16[44,1024]{1,0:T(8,128)(2,1)}, u32[]{:S(2)}) copy-start(bf16[44,1024]{1,0:T(8,128)(2,1)} %param.46) | copy-start | bytes 270340
  88.2 61.8 %copy-start.6 = (bf16[1024,44]{0,1:T(8,128)(2,1)S(1)}, bf16[1024,44]{0,1:T(8,128)(2,1)}, u32[]{:S(2)}) copy-start(bf16[1024,44]{0,1:T(8,128)(2,1)} %param.45) | copy-start | bytes 270340
  93.5 59.7 %all-to-all-start.4 = ((bf16[64,2,1024]{2,1,0:T(2,128)(2,1)}), bf16[64,2,1024]{2,1,0:T(2,128)(2,1)S(1)}, u32[]{:S(2)}, u32[]{:S(2)}) async-start(bf16[64,2,1024]{2,1,0:T(2,128)(2,1)} %reshape.137), calls=%async_computation.4 | async-start | bytes 524288 | tf_op jit(solution)/shard_map/all_to_all | solution.py:157
  150.0 14.9 %copy-start.15 = (bf16[16,2]{0,1:T(2,128)(2,1)S(1)}, bf16[16,2]{0,1:T(2,128)(2,1)}, u32[]{:S(2)}) copy-start(bf16[16,2]{0,1:T(2,128)(2,1)} %param.40) | copy-start | bytes 196
  153.2 56.9 %all-to-all-start.5 = ((bf16[64,8,1024]{2,1,0:T(8,128)(2,1)}), bf16[64,8,1024]{2,1,0:T(8,128)(2,1)S(1)}, u32[]{:S(2)}, u32[]{:S(2)}) async-start(bf16[64,8,1024]{2,1,0:T(8,128)(2,1)} %fusion.6), calls=%async_computation.5 | async-start | bytes 2097152 | tf_op jit(solution)/shard_map/all_to_all | solution.py:38
Sparse Core Ops, SparseCore 0:
  75.3 72.9 all-gather.1
where the time goes:
time: 219 us; the launch traced here: 218 us
  waiting for transfers between devices  103 us (47%)
  starting transfers between devices  54.6 us (25%)
  matrix products  17.7 us (8%)
  blocking collectives  17 us (8%)
  between operations  14.5 us (7%)
  other arithmetic  5.81 us (3%)
  local copies, waits for them, and re-layouts  5.25 us (2%)
    all_gather x1, waiting for transfers between devices, whole_of(): shard = lax.all_gather(shard, axis, axis=dim, tiled=True)  47.5 us
    all_to_all x1, waiting for transfers between devices, sent_and_summed(): lax.all_to_all(tiles, axis, split_axis=0, concat_axis=0, tiled=True)  44.8 us
    all_to_all x1, starting transfers between devices, local(): inbox = lax.all_to_all(outbox, EP, split_axis=0, concat_axis=0, tiled=True)  29 us
    all_gather x1, blocking collectives, whole_of(): shard = lax.all_gather(shard, axis, axis=dim, tiled=True)  12.7 us
    all_to_all x1, starting transfers between devices, sent_and_summed(): lax.all_to_all(tiles, axis, split_axis=0, concat_axis=0, tiled=True)  11.6 us
    all_to_all x1, waiting for transfers between devices, local(): inbox = lax.all_to_all(outbox, EP, split_axis=0, concat_axis=0, tiled=True)  8.55 us
    all_to_all x1, starting transfers between devices, local(): lax.all_to_all(results, EP, split_axis=0, concat_axis=0, tiled=True)  7.31 us
    all_to_all x2, starting transfers between devices, copy_for_each(): return lax.all_to_all(copies, axis, split_axis=0, concat_axis=0, tiled=True)  6.55 us
  transfers between devices with their start and end apart: 6, of which 5 were waited for; matrix products, arithmetic and copies ran while one was open for 5% of the time, Pallas kernels for 0%

commit v1 on v0

v1 whole, which is shorter than its diff:
```python
import functools

import jax
import jax.numpy as jnp
from jax import lax
from jax.experimental import pallas as pl
from jax.experimental.pallas import tpu as pltpu
from jax.sharding import PartitionSpec as P

MESH = pl.DeviceIdType.MESH
GRP_EP = ("grp", "ep")
GRP_EP_TP = ("grp", "ep", "tp")
NX = 4
SPAN = 2
PADDED = 48
LANES = 128

epsilon = 1e-06


def rms_norm(values, gains):
    floats = values.astype(jnp.float32)
    scaled = floats * lax.rsqrt(jnp.mean(floats * floats, axis=-1, keepdims=True) + epsilon)
    return (scaled * gains).astype(jnp.bfloat16)


def memory_step(query_rows, key_rows, value_rows, in_gate, forget_pre, matrix, norm_vec, old_max):
    log_forget = jax.nn.log_sigmoid(forget_pre)
    new_max = jnp.maximum(log_forget + old_max, in_gate)
    keep = jnp.exp(log_forget + old_max - new_max)
    write = jnp.exp(in_gate - new_max)
    matrix = (
        keep[..., None, None] * matrix
        + write[..., None, None] * key_rows[..., :, None] * value_rows[..., None, :]
    )
    norm_vec = keep[..., None] * norm_vec + write[..., None] * key_rows
    numer = jnp.einsum("bhd,bhde->bhe", query_rows, matrix, precision=lax.Precision.HIGHEST)
    denom = jnp.sum(query_rows * norm_vec, axis=-1)
    readout = numer / jnp.maximum(jnp.abs(denom), jnp.exp(-new_max))[..., None]
    return (readout, matrix, norm_vec, new_max)


def dot32(a, b, precision=None):
    return jnp.dot(a, b, preferred_element_type=jnp.float32, precision=precision)


def dot_nt(a, b):
    return lax.dot_general(a, b, (((1,), (1,)), ((), ())), preferred_element_type=jnp.float32)


def dot_tn(a, b):
    return lax.dot_general(a, b, (((0,), (0,)), ((), ())), preferred_element_type=jnp.float32)


def feed_kernel(
    nep,
    nx,
    span,
    all_width,
    tokens_ref,
    part_ref,
    routes_ref,
    scores_ref,
    gain_ref,
    blend_ref,
    block_ref,
    gate_hbm,
    up_hbm,
    down_hbm,
    out_ref,
    gate_v,
    up_v,
    down_v,
    part_in,
    resid_v,
    normed_v,
    relay,
    outbox,
    inbox,
    rows_v,
    half_out,
    half_in,
    backbox,
    homebox,
    acts_out,
    acts,
    blocks,
    dense_out,
    dense_in,
    swap_out,
    swap_in,
    local_sem,
    send_sem,
    recv_sem,
    block_send,
    block_recv,
):
    t = lax.axis_index("tp")
    me = lax.axis_index("ep")
    z, x = me // nx, me % nx
    nz = nep // nx
    members = nz // span
    own_rows, width = tokens_ref.shape
    half = width // 2
    pieces = half // LANES
    half_rows = own_rows // 2
    zi, zr = z // span, z % span
    my_block = zr * nx + x
    peers = nep - 1
    partner = {"tp": 1 - t}

    def remote(src, dst, send, recv, device):
        return pltpu.make_async_remote_copy(
            src_ref=src, dst_ref=dst, send_sem=send, recv_sem=recv, device_id=device, device_id_type=MESH
        )

    def await_bytes(ref, sem):
        pltpu.make_async_copy(ref, ref, sem).wait()

    barrier = pltpu.get_barrier_semaphore()

    @pl.loop(1, nep)
    def _(i):
        pl.semaphore_signal(barrier, inc=1, device_id={"ep": (me + i) % nep}, device_id_type=MESH)

    pl.semaphore_signal(barrier, inc=1, device_id=partner, device_id_type=MESH)
    loads = [
        pltpu.make_async_copy(src, dst, local_sem.at[i])
        for i, (src, dst) in enumerate(((gate_hbm.at[0], gate_v), (up_hbm.at[0], up_v), (down_hbm.at[0], down_v)))
    ]
    for load in loads:
        load.start()
    blocks[my_block] = block_ref[...]
    mine = pl.ds(pl.multiple_of(t * half, LANES), half)
    pl.semaphore_wait(barrier, nep)

    exchange = remote(part_ref, part_in, send_sem.at[0], recv_sem.at[0], partner)
    exchange.start()

    def block_copy(index, device, slot):
        ref = blocks.at[index, :, mine]
        return remote(ref, ref, block_send.at[slot], block_recv.at[index], device)

    if span == 2:
        pair = block_copy(my_block, {"ep": (z + 1 - 2 * zr) * nx + x}, 0)
        pair.start()
    exchange.wait()

    total = part_ref[...] + part_in[...]
    scale = lax.rsqrt(total[:, width : width + 1] / all_width + epsilon)
    resid = (tokens_ref[...].astype(jnp.float32) + scale * total[:, :width]).astype(jnp.bfloat16)
    resid32 = resid.astype(jnp.float32)
    resid_v[...] = resid32
    normed = rms_norm(resid32, gain_ref[...])
    normed_v[...] = normed.astype(jnp.float32)

    experts = lax.broadcasted_iota(jnp.int32, (own_rows, nep), 1)
    picks = [(routes_ref[:, k : k + 1] == experts).astype(jnp.float32) for k in range(2)]
    member = picks[0] + picks[1]
    row_at = lax.broadcasted_iota(jnp.int32, (own_rows, own_rows), 0)
    col_at = lax.broadcasted_iota(jnp.int32, (own_rows, own_rows), 1)
    earlier = (col_at < row_at).astype(jnp.float32)
    rank = dot32(earlier, member)
    chosen = [jnp.where(rank < 0.5, member, 0.0), jnp.where(rank < 0.5, 0.0, member)]

    def to_boxes(values, box):
        for slot in range(2):
            for c in range(pieces):
                relay[pl.ds(slot * pieces + c, nep, stride=2 * pieces), :] = values[slot][
                    :, c * LANES : (c + 1) * LANES
                ]
        box[...] = relay[...].reshape(nep, 2 * pieces, LANES).astype(jnp.bfloat16)

    def from_box(box, slot, c):
        return relay[pl.ds(slot * pieces + c, nep, stride=2 * pieces), :]

    own_half = normed_v[:, mine].astype(jnp.bfloat16)
    to_boxes([dot_tn(chosen[s].astype(jnp.bfloat16), own_half) for s in range(2)], outbox)

    def send_all(src, dst_at, sem):
        @pl.loop(0, nz)
        def _(k):
            away = nz // 2 + (2 * (k % 2) - 1) * ((k + 1) // 2)
            there_z = (z + away) % nz
            for j in range(nx):
                there = there_z * nx + (x + j) % nx

                @pl.when(there != me)
                def _():
                    remote(src.at[there], dst_at, send_sem.at[sem], recv_sem.at[sem], {"ep": there}).start()

    send_all(outbox, inbox.at[t, me], 1)
    inbox[t, me] = outbox[me]

    acts_out[...] = normed_v[pl.ds(pl.multiple_of(t * half_rows, half_rows), half_rows), :].astype(jnp.bfloat16)

    def block_to_x(index, base):
        copies = [block_copy(index, {"ep": z * nx + (x + j) % nx}, base + j) for j in range(1, nx)]
        for copy in copies:
            copy.start()
        return copies

    sent = block_to_x(my_block, 0)

    @pl.loop(1, members)
    def _(i):
        there = ((zi + i) % members) * span + zr
        remote(acts_out, acts.at[zi], send_sem.at[2], recv_sem.at[2], {"ep": there * nx + x}).start()

    acts[zi] = acts_out[...]

    def await_block(index):
        ref = blocks.at[index, :, mine]
        pltpu.make_async_copy(ref, ref, block_recv.at[index]).wait()

    if span == 2:
        other = (1 - zr) * nx + x
        await_block(other)
        sent += block_to_x(other, nx)

    box_bytes = inbox.at[0, pl.ds(0, peers)]
    await_bytes(box_bytes, recv_sem.at[1])
    box_swap = remote(inbox.at[t], inbox.at[t], send_sem.at[3], recv_sem.at[3], partner)
    box_swap.start()
    box_swap.wait_recv()

    for h in range(2):
        relay[...] = inbox[h].astype(jnp.float32).reshape(relay.shape)
        for slot in range(2):
            for c in range(pieces):
                at = h * half + c * LANES
                rows_v[slot * nep : (slot + 1) * nep, at : at + LANES] = from_box(relay, slot, c).astype(jnp.bfloat16)
    loads[0].wait()
    loads[1].wait()
    gate_val = dot32(rows_v[...], gate_v[...])
    up_val = dot32(rows_v[...], up_v[...])
    hidden = (jax.nn.silu(gate_val) * up_val).astype(jnp.bfloat16)
    loads[2].wait()
    for h in range(2):
        half_out[h] = dot32(hidden, down_v[:, h * half : (h + 1) * half]).astype(jnp.bfloat16)
    half_swap = remote(half_out.at[1 - t], half_in, send_sem.at[4], recv_sem.at[4], partner)
    half_swap.start()

    theirs = pl.ds(pl.multiple_of((1 - t) * half, LANES), half)

    def block_swap(index):
        ref = blocks.at[index, :, mine]
        return remote(ref, ref, block_send.at[2 * nx + index], block_recv.at[span * nx + index], partner)

    for i in range(1, span * nx):
        index = (my_block + i) % (span * nx)
        if not (span == 2 and i == nx):
            await_block(index)
        block_swap(index).start()

    half_swap.wait_recv()
    summed = (half_out[t].astype(jnp.float32) + half_in[...].astype(jnp.float32)).astype(jnp.bfloat16)
    summed = summed.astype(jnp.float32)
    await_bytes(box_bytes, send_sem.at[1])
    to_boxes([summed[s * nep : (s + 1) * nep] for s in range(2)], backbox)
    send_all(backbox, homebox.at[me], 5)
    homebox[me] = backbox[me]

    for i in range(1, span * nx):
        index = (my_block + i) % (span * nx)
        ref = blocks.at[index, :, theirs]
        pltpu.make_async_copy(ref, ref, block_recv.at[span * nx + index]).wait()
    act_bytes = acts.at[pl.ds(0, members - 1)]
    await_bytes(act_bytes, recv_sem.at[2])
    dense_rows = acts[...].astype(jnp.float32).reshape(members * half_rows, width).astype(jnp.bfloat16)
    dense = jnp.zeros((members * half_rows, width), jnp.float32)
    for index in range(span * nx):
        left = dot_nt(dense_rows, blocks[index, 0:PADDED, :])
        right = dot_nt(dense_rows, blocks[index, PADDED : 2 * PADDED, :])
        units = (jax.nn.silu(left) * right).astype(jnp.bfloat16)
        dense = dense + dot32(units, blocks[index, 2 * PADDED : 3 * PADDED, :])
    dense_out[...] = dense.reshape(members, half_rows, width).astype(jnp.bfloat16)

    @pl.loop(1, members)
    def _(i):
        mi = (zi + i) % members
        there = mi * span + zr
        remote(dense_out.at[mi], dense_in.at[zi], send_sem.at[6], recv_sem.at[6], {"ep": there * nx + x}).start()

    dense_in[zi] = dense_out[zi]

    scores = scores_ref[...].astype(jnp.float32)
    top = jnp.max(scores, axis=-1, keepdims=True)
    powers = jnp.exp(scores - top)
    weights = powers / jnp.sum(powers, axis=-1, keepdims=True)
    weight_of = weights[:, 0:1] * picks[0] + weights[:, 1:2] * picks[1]
    await_bytes(homebox.at[pl.ds(0, peers)], recv_sem.at[5])
    relay[...] = homebox[...].astype(jnp.float32).reshape(relay.shape)
    routed = []
    for c in range(pieces):
        piece = jnp.zeros((own_rows, LANES), jnp.float32)
        for slot in range(2):
            taken = jnp.where(chosen[slot] > 0.5, weight_of, 0.0)
            piece = piece + dot32(taken, from_box(relay, slot, c), lax.Precision.HIGHEST)
        routed.append(piece)
    routed = jnp.concatenate(routed, axis=1)
    for h in range(2):
        swap_out[h] = routed[h * half_rows : (h + 1) * half_rows]
    swap = remote(swap_out.at[1 - t], swap_in, send_sem.at[7], recv_sem.at[7], partner)
    swap.start()

    home = pl.ds(pl.multiple_of(t * half_rows, half_rows), half_rows)
    own_normed = normed_v[home, :]
    blend = jax.nn.sigmoid(jnp.sum(own_normed * blend_ref[...], axis=-1, keepdims=True))
    await_bytes(dense_in.at[pl.ds(0, members - 1)], recv_sem.at[6])
    base = resid_v[home, :] + blend * jnp.sum(dense_in[...].astype(jnp.float32), axis=0)
    resid_v[home, :] = base
    swap.wait_recv()
    out_ref[:, mine] = (resid_v[home, mine] + swap_out[t]).astype(jnp.bfloat16)
    out_ref[:, theirs] = (resid_v[home, theirs] + swap_in[...]).astype(jnp.bfloat16)

    await_bytes(act_bytes, send_sem.at[2])
    box_swap.wait_send()
    half_swap.wait_send()
    await_bytes(box_bytes, send_sem.at[5])
    await_bytes(dense_in.at[pl.ds(0, members - 1)], send_sem.at[6])
    swap.wait_send()
    if span == 2:
        pair.wait_send()
    for copy in sent:
        copy.wait_send()
    for i in range(1, span * nx):
        block_swap((my_block + i) % (span * nx)).wait_send()


def feed(nep, nx, span, all_width, tokens, part, routes, scores, gain, blend, block, gate, up, down):
    own_rows, width = tokens.shape
    half, half_rows = width // 2, own_rows // 2
    pieces = half // LANES
    members = nep // nx // span
    hidden = gate.shape[2]
    bf16, f32 = jnp.bfloat16, jnp.float32
    vmem = pl.BlockSpec(memory_space=pltpu.VMEM)
    anywhere = pl.BlockSpec(memory_space=pl.ANY)
    box = (nep, 2 * pieces, LANES)
    return pl.pallas_call(
        functools.partial(feed_kernel, nep, nx, span, all_width),
        out_shape=jax.ShapeDtypeStruct((half_rows, width), bf16),
        in_specs=[vmem] * 7 + [anywhere] * 3,
        out_specs=vmem,
        scratch_shapes=[
            pltpu.VMEM((width, hidden), bf16),
            pltpu.VMEM((width, hidden), bf16),
            pltpu.VMEM((hidden, width), bf16),
            pltpu.VMEM((own_rows, width + LANES), f32),
            pltpu.VMEM((own_rows, width), f32),
            pltpu.VMEM((own_rows, width), f32),
            pltpu.VMEM((nep * 2 * pieces, LANES), f32),
            pltpu.VMEM(box, bf16),
            pltpu.VMEM((2, *box), bf16),
            pltpu.VMEM((2 * nep, width), bf16),
            pltpu.VMEM((2, 2 * nep, half), bf16),
            pltpu.VMEM((2 * nep, half), bf16),
            pltpu.VMEM(box, bf16),
            pltpu.VMEM(box, bf16),
            pltpu.VMEM((half_rows, width), bf16),
            pltpu.VMEM((members, half_rows, width), bf16),
            pltpu.VMEM((span * nx, 3 * PADDED, width), bf16),
            pltpu.VMEM((members, half_rows, width), bf16),
            pltpu.VMEM((members, half_rows, width), bf16),
            pltpu.VMEM((2, half_rows, half), f32),
            pltpu.VMEM((half_rows, half), f32),
            pltpu.SemaphoreType.DMA((3,)),
            pltpu.SemaphoreType.DMA((8,)),
            pltpu.SemaphoreType.DMA((8,)),
            pltpu.SemaphoreType.DMA((2 * nx + span * nx,)),
            pltpu.SemaphoreType.DMA((2 * span * nx,)),
        ],
        compiler_params=pltpu.CompilerParams(
            collective_id=0, has_side_effects=True, vmem_limit_bytes=48 * 1024 * 1024
        ),
        name="feed",
    )(tokens, part, routes, scores, gain, blend, block, gate, up, down)


def local(
    nx,
    span,
    tokens,
    query_weight,
    key_weight,
    value_weight,
    outgate_weight,
    ingate_weight,
    forget_weight,
    forget_bias,
    head_gain,
    merge_weight,
    mixer_gain,
    feed_gain,
    memory_matrix,
    memory_norm,
    memory_max,
    routes,
    route_scores,
    expert_gate,
    expert_up,
    expert_down,
    dense_left,
    dense_right,
    dense_down,
    blend_weight,
):
    own_rows = tokens.shape[0]
    heads_here = forget_bias.shape[0]
    head_size = head_gain.shape[1]
    width_here = heads_here * head_size
    normed = rms_norm(tokens, mixer_gain)

    def project(weight):
        return jnp.dot(normed, weight, preferred_element_type=jnp.float32)

    query = project(query_weight).reshape(own_rows, heads_here, head_size)
    key_rows = project(key_weight).reshape(own_rows, heads_here, head_size) * head_size ** (-0.5)
    value_rows = project(value_weight).reshape(own_rows, heads_here, head_size)
    outgate_rows = project(outgate_weight).reshape(own_rows, heads_here, head_size)
    in_gate = project(ingate_weight)
    forget_pre = project(forget_weight) + forget_bias
    readout, matrix, norm_vec, new_max = memory_step(
        query, key_rows, value_rows, in_gate, forget_pre, memory_matrix, memory_norm, memory_max
    )
    energy = jnp.sum(readout * readout, axis=(1, 2))
    gated = (
        (readout * head_gain * jax.nn.sigmoid(outgate_rows))
        .reshape(own_rows, width_here)
        .astype(jnp.bfloat16)
    )
    head_part = jnp.dot(gated, merge_weight, preferred_element_type=jnp.float32)
    part = jnp.concatenate([head_part, jnp.broadcast_to(energy[:, None], (own_rows, LANES))], axis=1)

    def padded(rows):
        return jnp.pad(rows, ((0, PADDED - rows.shape[0]), (0, 0)))

    block = jnp.concatenate([padded(dense_left.T), padded(dense_right.T), padded(dense_down)], axis=0)
    layer_out = feed(
        lax.axis_size("ep"),
        nx,
        span,
        width_here * lax.axis_size("tp"),
        tokens,
        part,
        routes,
        route_scores,
        feed_gain[None, :],
        blend_weight[None, :],
        block,
        expert_gate,
        expert_up,
        expert_down,
    )
    return (layer_out, matrix, norm_vec, new_max)


def build(mesh, nx, span):
    return jax.shard_map(
        functools.partial(local, nx, span),
        mesh=mesh,
        in_specs=(
            P(GRP_EP, None),
            P(None, "tp"),
            P(None, "tp"),
            P(None, "tp"),
            P(None, "tp"),
            P(None, "tp"),
            P(None, "tp"),
            P("tp"),
            P("tp", None),
            P("tp", None),
            P(),
            P(),
            P(GRP_EP, "tp", None, None),
            P(GRP_EP, "tp", None),
            P(GRP_EP, "tp"),
            P(GRP_EP, None),
            P(GRP_EP, None),
            P("ep", None, "tp"),
            P("ep", None, "tp"),
            P("ep", "tp", None),
            P(None, "ep"),
            P(None, "ep"),
            P("ep", None),
            P(),
        ),
        out_specs=(
            P(GRP_EP_TP, None),
            P(GRP_EP, "tp", None, None),
            P(GRP_EP, "tp", None),
            P(GRP_EP, "tp"),
        ),
        check_vma=False,
    )


def solution(mesh):
    return build(mesh, NX, SPAN)
```

time: 219 us -> 84.1 us (0.38)
  waiting for transfers between devices: 103 us -> 0 us
  Pallas kernels: 0 us -> 64.2 us
  starting transfers between devices: 54.6 us -> 0 us
  blocking collectives: 17 us -> 0 us
  between operations: 14.5 us -> 0.89 us
  matrix products: 17.7 us -> 9.84 us
    pallas_call x0 -> x1, Pallas kernels: none -> 64.2 us  [feed(): pl.pallas_call(functools.partial(feed_kernel, nep, nx, span, all_width),...]
    all_to_all x5 -> x0, waiting for transfers between devices: 55.4 us -> none  [the longest x1 44.8 us: sent_and_summed(): lax.all_to_all(tiles, axis, split_axis=0, concat_axis=0, tiled=True)]
    all_to_all x5 -> x0, starting transfers between devices: 54.5 us -> none  [the longest x1 29 us: local(): inbox = lax.all_to_all(outbox, EP, split_axis=0, concat_axis=0, tiled=True)]
    all_gather x1 -> x0, waiting for transfers between devices: 47.5 us -> none  [whole_of(): shard = lax.all_gather(shard, axis, axis=dim, tiled=True)]
    all_gather x1 -> x0, blocking collectives: 12.7 us -> none  [whole_of(): shard = lax.all_gather(shard, axis, axis=dim, tiled=True)]
    dot_general x6 -> x0, matrix products: 9.59 us -> none  [the longest x1 3.15 us: dense_block(): return jnp.dot(dense_hidden, dense_down, preferred_element_type=jnp.float32)]
    all_to_all x1 -> x0, blocking collectives: 4.3 us -> none  [copy_for_each(): return lax.all_to_all(copies, axis, split_axis=0, concat_axis=0, tiled=True)]
    unnamed x33 -> x37, local copies, waits for them, and re-layouts: 1.42 us -> 3.87 us
  transfers between devices with their start and end apart: 6 -> 0, of which waited for: 5 -> 0; matrix products, arithmetic and copies ran while one was open for 5% -> 0% of each run, Pallas kernels for 0% -> 0%
where the time goes in v1:
time: 84.1 us; the launch traced here: 83.8 us
  Pallas kernels  64.2 us (76%)
  matrix products  9.84 us (12%)
  other arithmetic  4.51 us (5%)
  local copies, waits for them, and re-layouts  4.36 us (5%)
  between operations  0.89 us (1%)
    pallas_call x1, Pallas kernels, feed(): pl.pallas_call(functools.partial(feed_kernel, nep, nx, span, all_width),...  64.2 us
    dot_general x6, matrix products, project(): return jnp.dot(normed, weight, preferred_element_type=jnp.float32)  6.07 us
    unnamed x37, local copies, waits for them, and re-layouts  3.87 us
    dot_general x1, matrix products, memory_step(): jnp.einsum('bhd,bhde->bhe', query_rows, matrix, precision=lax.Precision.H...  3.58 us
    add x1, other arithmetic, memory_step(): keep[..., None, None] * matrix  1.71 us

profile of v1, /device:TPU:40, one launch (start us, length us, event | category | flops | bytes accessed | tf_op | source)
XLA Modules:
  0.0 83.8 jit_solution(12483338629463980892)
XLA Ops:
  0.6 0.0 copy-start
  0.6 0.0 copy-start.7
  0.7 1.0 %fusion.10 = f32[16]{0:T(128)S(1)} fusion(bf16[16,1024]{1,0:T(8,128)(2,1)} %tokens_ref.1), kind=kLoop, calls=%fused_computation.20 | loop fusion | flops 49136 | bytes 32832 | tf_op jit(solution)/shard_map/reduce_sum | solution.py:23
  1.7 1.0 %fusion.23 = f32[16,2]{0,1:T(2,128)S(1)} fusion(bf16[1024,2]{0,1:T(2,128)(2,1)} %param.29, bf16[16,1024]{1,0:T(8,128)(2,1)} %tokens_ref.1, f32[1024]{0:T(1024)} %param.34, f32[16]{0:T(128)S(1)} %add_rsqrt_fusion), kind=kOutput, calls=%fused_computation.41 | convolution fusion | flops 131072 | bytes 41152 | tf_op jit(solution)/shard_map/dot_general | solution.py:416
  2.7 1.0 %subtract_exponential_fusion = (f32[16,2]{0,1:T(2,128)S(1)}, f32[16,2]{0,1:T(2,128)S(1)}) fusion(f32[16,2]{0,1:T(2,128)S(1)} %fusion.23, f32[16,2]{0,1:T(2,128)} %param.38, f32[2]{0:T(128)} %param.31, bf16[1024,2]{0,1:T(2,128)(2,1)} %param.30, bf16[16,1024]{1,0:T(8,128)(2,1)} %tokens_ref.1, f32[1024]{0:T(1024)} %param.34, f32[16]{0:T(128)S(1)} %add_rsqrt_fusion), kind=kOutput, calls=%fused_computation.37 | convolution fusion | flops 131456 | bytes 41544 | tf_op jit(solution)/shard_map/dot_general | solution.py:416
  3.7 0.0 copy-start.13
  3.7 0.1 copy.35
  3.8 0.1 copy.34
  3.9 1.3 %fusion.26 = f32[16,256]{1,0:T(8,128)S(1)} fusion(bf16[1024,256]{1,0:T(8,128)(2,1)} %param.25, bf16[16,1024]{1,0:T(8,128)(2,1)} %tokens_ref.1, f32[1024]{0:T(1024)} %param.34, f32[16]{0:T(128)S(1)} %add_rsqrt_fusion), kind=kOutput, calls=%fused_computation.42 | convolution fusion | flops 8454144 | bytes 577600 | tf_op jit(solution)/shard_map/dot_general | solution.py:416
  5.2 1.3 %fusion.21 = f32[16,256]{1,0:T(8,128)S(1)} fusion(bf16[1024,256]{1,0:T(8,128)(2,1)} %param.26, bf16[16,1024]{1,0:T(8,128)(2,1)} %tokens_ref.1, f32[1024]{0:T(1024)} %param.34, f32[16]{0:T(128)S(1)} %add_rsqrt_fusion), kind=kOutput, calls=%fused_computation.40 | convolution fusion | flops 8454144 | bytes 577600 | tf_op jit(solution)/shard_map/dot_general | solution.py:416
  6.5 1.4 %multiply_reduce_fusion.1 = (f32[16,2]{1,0:T(8,128)S(1)}, f32[16,2,128]{2,1,0:T(2,128)}, f32[16,2,128]{2,1,0:T(2,128)S(1)}) fusion(f32[16,2,128]{2,1,0:T(2,128)S(1)} %reshape.49, f32[16,2,128]{2,1,0:T(2,128)} %param.37, f32[16,2]{1,0:T(8,128)S(1)} %copy.34, f32[16,2,128]{2,1,0:T(2,128)S(1)} %reshape.50, f32[16,2]{1,0:T(8,128)S(1)} %copy.35), kind=kLoop, calls=%fused_computation.25 | loop fusion | flops 20448 | bytes 82304 | tf_op jit(solution)/shard_map/reduce_sum | solution.py:38
  7.9 1.3 %fusion.19 = f32[16,256]{1,0:T(8,128)S(1)} fusion(bf16[1024,256]{1,0:T(8,128)(2,1)} %param.27, bf16[16,1024]{1,0:T(8,128)(2,1)} %tokens_ref.1, f32[1024]{0:T(1024)} %param.34, f32[16]{0:T(128)S(1)} %add_rsqrt_fusion), kind=kOutput, calls=%fused_computation.39 | convolution fusion | flops 8454144 | bytes 577600 | tf_op jit(solution)/shard_map/dot_general | solution.py:416
  9.3 0.0 copy-done.7
  9.3 1.7 %multiply_add_fusion = f32[16,2,128,128]{3,2,1,0:T(8,128)} fusion(f32[16,2,128,128]{3,2,1,0:T(8,128)S(1)} %copy-done.7, f32[16,2,128]{2,1,0:T(2,128)S(1)} %mul.103, f32[16,2,128]{2,1,0:T(2,128)S(1)} %get-tuple-element.8, f32[16,2]{1,0:T(8,128)S(1)} %copy.34), kind=kLoop, calls=%fused_computation | loop fusion | flops 1572864 | bytes 4227200 | tf_op jit(solution)/shard_map/add | solution.py:33
  11.0 0.0 copy-start.4
  11.0 0.0 copy-start.8
  11.0 0.0 copy-start.12
  11.0 0.0 copy-start.14
  11.0 0.0 copy-start.9
  11.0 0.0 copy-start.10
  11.0 0.0 copy-start.11
  11.0 0.0 copy-start.15
  11.1 0.0 copy-start.16
  11.1 0.0 copy-start.1
  11.1 0.0 copy-start.5
  11.1 0.0 copy-start.6
  11.1 3.6 %fusion.28 = f32[16,2,1,128]{3,2,1,0:T(1,128)S(1)} fusion(f32[16,2,128,1]{2,3,1,0:T(1,128)S(1)} %bitcast.24, f32[16,2,128,128]{3,2,1,0:T(8,128)} %multiply_add_fusion), kind=kOutput, calls=%fused_computation.43 | convolution fusion | flops 6291456 | bytes 2129920 | tf_op jit(solution)/shard_map/bhd,bhde->bhe/dot_general | solution.py:37
  14.7 0.1 copy.37
  14.8 0.0 copy-done.13
  14.8 0.1 copy.38
  14.9 0.0 copy-done.4
  14.9 0.0 copy-done.8
  14.9 0.0 copy-done.12
  14.9 0.2 fusion.2
  15.1 0.0 copy-done.14
  15.1 0.1 multiply_convert_fusion
  15.2 0.0 copy-done
  15.2 0.2 fusion.13
  15.4 0.2 multiply_reduce_fusion
  15.6 0.1 broadcast_in_dim.6
  15.7 0.0 copy-done.9
  15.7 0.0 copy-done.10
  15.7 0.0 copy-done.11
  15.8 0.0 copy-done.15
  15.8 0.1 copy.39.routes_ref
  15.9 0.0 copy-done.16
  15.9 0.1 copy.40.scores_ref
  16.0 0.0 copy-done.1
  16.0 0.0 copy-done.5
  16.0 0.0 copy-done.6
  16.0 0.0 copy-start.2
  16.0 1.5 %copy-done.2 = bf16[1,1024,896]{2,1,0:T(8,128)(2,1)S(1)} copy-done((bf16[1,1024,896]{2,1,0:T(8,128)(2,1)S(1)}, bf16[1,1024,896]{2,1,0:T(8,128)(2,1)}, u32[]{:S(2)}) %copy-start.2) | copy-done | bytes 1835032
  17.5 0.0 copy-start.3
  17.5 1.5 %copy-done.3 = bf16[1,896,1024]{2,1,0:T(8,128)(2,1)S(1)} copy-done((bf16[1,896,1024]{2,1,0:T(8,128)(2,1)S(1)}, bf16[1,896,1024]{2,1,0:T(8,128)(2,1)}, u32[]{:S(2)}) %copy-start.3) | copy-done | bytes 1835032
  19.0 64.2 %feed.1 = bf16[8,1024]{1,0:T(8,128)(2,1)S(1)} custom-call(bf16[16,1024]{1,0:T(8,128)(2,1)S(1)} %copy-done.4, f32[16,1152]{1,0:T(8,128)S(1)} %pad_maximum_fusion.part_ref, s32[16,2]{1,0:T(8,128)S(1)} %copy.39.routes_ref, bf16[16,2]{1,0:T(8,128)(2,1)S(1)} %copy.40.scores_ref, f32[1,1024]{1,0:T(1,128)S(1)} %bitcast.20, f32[1,1024]{1,0:T(1,128)S(1)} %bitcast.21, ...), custom_call_target="tpu_custom_call" | custom-call | tf_op jit(solution)/shard_map/feed/pallas_call | solution.py:341
  83.1 0.6 copy.49
  (10 shorter events, 0.1 us)
Async XLA Ops:
  0.6 14.6 %copy-start = (bf16[256,1024]{1,0:T(8,128)(2,1)S(1)}, bf16[256,1024]{1,0:T(8,128)(2,1)}, u32[]{:S(2)}) copy-start(bf16[256,1024]{1,0:T(8,128)(2,1)} %param.33) | copy-start | bytes 1572868
  0.6 8.6 %copy-start.7 = (f32[16,2,128,128]{3,2,1,0:T(8,128)S(1)}, f32[16,2,128,128]{3,2,1,0:T(8,128)}, u32[]{:S(2)}) copy-start(f32[16,2,128,128]{3,2,1,0:T(8,128)} %param.36) | copy-start | bytes 6291460
  3.7 11.1 %copy-start.13 = (f32[16,2]{0,1:T(2,128)}, f32[16,2]{0,1:T(2,128)S(1)}, u32[]{:S(2)}) copy-start(f32[16,2]{0,1:T(2,128)S(1)} %get-tuple-element.18) | copy-start | bytes 388
  11.0 3.9 %copy-start.4 = (bf16[16,1024]{1,0:T(8,128)(2,1)S(1)}, bf16[16,1024]{1,0:T(8,128)(2,1)}, u32[]{:S(2)}) copy-start(bf16[16,1024]{1,0:T(8,128)(2,1)} %tokens_ref.1) | copy-start | bytes 98308
  11.0 3.9 %copy-start.8 = (bf16[1024,256]{1,0:T(8,128)(2,1)S(1)}, bf16[1024,256]{1,0:T(8,128)(2,1)}, u32[]{:S(2)}) copy-start(bf16[1024,256]{1,0:T(8,128)(2,1)} %param.28) | copy-start | bytes 1572868
  11.0 3.9 %copy-start.12 = (f32[1024]{0:T(1024)S(1)}, f32[1024]{0:T(1024)}, u32[]{:S(2)}) copy-start(f32[1024]{0:T(1024)} %param.34) | copy-start | bytes 12292
  11.0 4.2 %copy-start.14 = (f32[2,128]{1,0:T(2,128)S(1)}, f32[2,128]{1,0:T(2,128)}, u32[]{:S(2)}) copy-start(f32[2,128]{1,0:T(2,128)} %param.32) | copy-start | bytes 3076
  11.0 4.7 %copy-start.9 = (bf16[44,1024]{1,0:T(8,128)(2,1)S(1)}, bf16[44,1024]{1,0:T(8,128)(2,1)}, u32[]{:S(2)}) copy-start(bf16[44,1024]{1,0:T(8,128)(2,1)} %param.46) | copy-start | bytes 270340
  11.0 4.7 %copy-start.10 = (bf16[1024,44]{0,1:T(8,128)(2,1)S(1)}, bf16[1024,44]{0,1:T(8,128)(2,1)}, u32[]{:S(2)}) copy-start(bf16[1024,44]{0,1:T(8,128)(2,1)} %param.45) | copy-start | bytes 270340
  11.0 4.7 %copy-start.11 = (bf16[1024,44]{0,1:T(8,128)(2,1)S(1)}, bf16[1024,44]{0,1:T(8,128)(2,1)}, u32[]{:S(2)}) copy-start(bf16[1024,44]{0,1:T(8,128)(2,1)} %param.44) | copy-start | bytes 270340
  11.0 4.7 %copy-start.15 = (s32[16,2]{0,1:T(2,128)S(1)}, s32[16,2]{0,1:T(2,128)}, u32[]{:S(2)}) copy-start(s32[16,2]{0,1:T(2,128)} %param.39) | copy-start | bytes 388
  11.1 4.8 %copy-start.16 = (bf16[16,2]{0,1:T(2,128)(2,1)S(1)}, bf16[16,2]{0,1:T(2,128)(2,1)}, u32[]{:S(2)}) copy-start(bf16[16,2]{0,1:T(2,128)(2,1)} %param.40) | copy-start | bytes 196
  11.1 4.9 %copy-start.1 = (bf16[1,1024,896]{2,1,0:T(8,128)(2,1)S(1)}, bf16[1,1024,896]{2,1,0:T(8,128)(2,1)}, u32[]{:S(2)}) copy-start(bf16[1,1024,896]{2,1,0:T(8,128)(2,1)} %gate_hbm.1) | copy-start | bytes 5505028
  11.1 4.9 %copy-start.5 = (f32[1024]{0:T(1024)S(1)}, f32[1024]{0:T(1024)}, u32[]{:S(2)}) copy-start(f32[1024]{0:T(1024)} %param.35) | copy-start | bytes 12292
  11.1 4.9 %copy-start.6 = (f32[1024]{0:T(1024)S(1)}, f32[1024]{0:T(1024)}, u32[]{:S(2)}) copy-start(f32[1024]{0:T(1024)} %param.47) | copy-start | bytes 12292
  16.0 1.5 %copy-start.2 = (bf16[1,1024,896]{2,1,0:T(8,128)(2,1)S(1)}, bf16[1,1024,896]{2,1,0:T(8,128)(2,1)}, u32[]{:S(2)}) copy-start(bf16[1,1024,896]{2,1,0:T(8,128)(2,1)} %up_hbm.1) | copy-start | bytes 5505028
  17.5 1.5 %copy-start.3 = (bf16[1,896,1024]{2,1,0:T(8,128)(2,1)S(1)}, bf16[1,896,1024]{2,1,0:T(8,128)(2,1)}, u32[]{:S(2)}) copy-start(bf16[1,896,1024]{2,1,0:T(8,128)(2,1)} %down_hbm.1) | copy-start | bytes 5505028

commit v2 on v1

--- a/solution.py
+++ b/solution.py
@@ -13,6 +13,7 @@
 NX = 4
 SPAN = 2
 PADDED = 48
+CHUNKS = 4
 LANES = 128
 
 epsilon = 1e-06
@@ -22,22 +23,6 @@
     floats = values.astype(jnp.float32)
     scaled = floats * lax.rsqrt(jnp.mean(floats * floats, axis=-1, keepdims=True) + epsilon)
     return (scaled * gains).astype(jnp.bfloat16)
-
-
-def memory_step(query_rows, key_rows, value_rows, in_gate, forget_pre, matrix, norm_vec, old_max):
-    log_forget = jax.nn.log_sigmoid(forget_pre)
-    new_max = jnp.maximum(log_forget + old_max, in_gate)
-    keep = jnp.exp(log_forget + old_max - new_max)
-    write = jnp.exp(in_gate - new_max)
-    matrix = (
-        keep[..., None, None] * matrix
-        + write[..., None, None] * key_rows[..., :, None] * value_rows[..., None, :]
-    )
-    norm_vec = keep[..., None] * norm_vec + write[..., None] * key_rows
-    numer = jnp.einsum("bhd,bhde->bhe", query_rows, matrix, precision=lax.Precision.HIGHEST)
-    denom = jnp.sum(query_rows * norm_vec, axis=-1)
-    readout = numer / jnp.maximum(jnp.abs(denom), jnp.exp(-new_max))[..., None]
-    return (readout, matrix, norm_vec, new_max)
 
 
 def dot32(a, b, precision=None):
@@ -58,16 +43,35 @@
     span,
     all_width,
     tokens_ref,
-    part_ref,
     routes_ref,
     scores_ref,
+    mixer_ref,
     gain_ref,
     blend_ref,
     block_ref,
+    inforget_ref,
+    bias_ref,
+    head_gain_ref,
+    norm_ref,
+    max_ref,
+    query_hbm,
+    key_hbm,
+    value_hbm,
+    outgate_hbm,
+    merge_hbm,
+    matrix_hbm,
     gate_hbm,
     up_hbm,
     down_hbm,
     out_ref,
+    new_matrix_hbm,
+    new_norm_ref,
+    new_max_ref,
+    project_v,
+    merge_v,
+    matrix_v,
+    numer_v,
+    part_ref,
     gate_v,
     up_v,
     down_v,
@@ -124,14 +128,68 @@
         pl.semaphore_signal(barrier, inc=1, device_id={"ep": (me + i) % nep}, device_id_type=MESH)
 
     pl.semaphore_signal(barrier, inc=1, device_id=partner, device_id_type=MESH)
-    loads = [
-        pltpu.make_async_copy(src, dst, local_sem.at[i])
-        for i, (src, dst) in enumerate(((gate_hbm.at[0], gate_v), (up_hbm.at[0], up_v), (down_hbm.at[0], down_v)))
+    moves = [(src, project_v.at[i]) for i, src in enumerate((query_hbm, key_hbm, value_hbm, outgate_hbm))]
+    chunk = own_rows // CHUNKS
+    for c in range(CHUNKS):
+        rows = pl.ds(c * chunk, chunk)
+        moves.append((matrix_hbm.at[rows], matrix_v.at[rows]))
+    moves += [(merge_hbm, merge_v), (gate_hbm.at[0], gate_v), (up_hbm.at[0], up_v), (down_hbm.at[0], down_v)]
+    loads = [pltpu.make_async_copy(src, dst, local_sem.at[i]) for i, (src, dst) in enumerate(moves)]
+    stores = [
+        pltpu.make_async_copy(dst, new_matrix_hbm.at[pl.ds(c * chunk, chunk)], local_sem.at[len(loads) + c])
+        for c, (_, dst) in enumerate(moves[4 : 4 + CHUNKS])
     ]
     for load in loads:
         load.start()
     blocks[my_block] = block_ref[...]
     mine = pl.ds(pl.multiple_of(t * half, LANES), half)
+
+    heads, head = head_gain_ref.shape
+    first = rms_norm(tokens_ref[...], mixer_ref[...])
+    gates = dot32(first, inforget_ref[...])
+    in_gate = gates[:, 0:heads]
+    log_forget = jax.nn.log_sigmoid(gates[:, heads : 2 * heads] + bias_ref[...])
+    old_max = max_ref[...]
+    new_max = jnp.maximum(log_forget + old_max, in_gate)
+    new_max_ref[...] = new_max
+    keep = jnp.exp(log_forget + old_max - new_max)
+    write = jnp.exp(in_gate - new_max)
+    floor = jnp.exp(-new_max)
+    projected = []
+    for i in range(4):
+        loads[i].wait()
+        projected.append(dot32(first, project_v[i]))
+    by_head = [[p[:, h * head : (h + 1) * head] for h in range(heads)] for p in projected]
+    queries, keys, values, outgates = by_head
+    written = [write[:, h : h + 1] * (keys[h] * head ** (-0.5)) for h in range(heads)]
+    columns = jnp.concatenate(queries + written, axis=0).T
+    norms = []
+    for h in range(heads):
+        norm = keep[:, h : h + 1] * norm_ref[:, h * head : (h + 1) * head] + written[h]
+        new_norm_ref[:, h * head : (h + 1) * head] = norm
+        norms.append(norm)
+    for b in range(own_rows):
+        if b % chunk == 0:
+            loads[4 + b // chunk].wait()
+        for h in range(heads):
+            at = h * own_rows + b
+            to = heads * own_rows + at
+            fresh = keep[b : b + 1, h : h + 1] * matrix_v[b, h] + columns[:, to : to + 1] * values[h][b : b + 1, :]
+            matrix_v[b, h] = fresh
+            numer_v[h, b : b + 1, :] = jnp.sum(columns[:, at : at + 1] * fresh, axis=0, keepdims=True)
+        if b % chunk == chunk - 1:
+            stores[b // chunk].start()
+    energy = jnp.zeros((own_rows, 1), jnp.float32)
+    gated = []
+    for h in range(heads):
+        denom = jnp.sum(queries[h] * norms[h], axis=-1, keepdims=True)
+        readout = numer_v[h] / jnp.maximum(jnp.abs(denom), floor[:, h : h + 1])
+        energy = energy + jnp.sum(readout * readout, axis=-1, keepdims=True)
+        gated.append((readout * head_gain_ref[h : h + 1, :] * jax.nn.sigmoid(outgates[h])).astype(jnp.bfloat16))
+    loads[4 + CHUNKS].wait()
+    part_ref[:, 0:width] = dot32(jnp.concatenate(gated, axis=1), merge_v[...])
+    part_ref[:, width : width + LANES] = jnp.broadcast_to(energy, (own_rows, LANES))
+    loads = loads[5 + CHUNKS :]
     pl.semaphore_wait(barrier, nep)
 
     exchange = remote(part_ref, part_in, send_sem.at[0], recv_sem.at[0], partner)
@@ -314,6 +372,8 @@
     out_ref[:, mine] = (resid_v[home, mine] + swap_out[t]).astype(jnp.bfloat16)
     out_ref[:, theirs] = (resid_v[home, theirs] + swap_in[...]).astype(jnp.bfloat16)
 
+    for store in stores:
+        store.wait()
     await_bytes(act_bytes, send_sem.at[2])
     box_swap.wait_send()
     half_swap.wait_send()
@@ -328,22 +388,34 @@
         block_swap((my_block + i) % (span * nx)).wait_send()
 
 
-def feed(nep, nx, span, all_width, tokens, part, routes, scores, gain, blend, block, gate, up, down):
-    own_rows, width = tokens.shape
+def feed(nep, nx, span, all_width, resident, streamed):
+    own_rows, width = resident[0].shape
     half, half_rows = width // 2, own_rows // 2
     pieces = half // LANES
     members = nep // nx // span
-    hidden = gate.shape[2]
+    hidden = streamed[6].shape[2]
+    here = streamed[0].shape[1]
+    matrix = streamed[5]
     bf16, f32 = jnp.bfloat16, jnp.float32
     vmem = pl.BlockSpec(memory_space=pltpu.VMEM)
-    anywhere = pl.BlockSpec(memory_space=pl.ANY)
+    hbm = pl.BlockSpec(memory_space=pltpu.HBM)
     box = (nep, 2 * pieces, LANES)
     return pl.pallas_call(
         functools.partial(feed_kernel, nep, nx, span, all_width),
-        out_shape=jax.ShapeDtypeStruct((half_rows, width), bf16),
-        in_specs=[vmem] * 7 + [anywhere] * 3,
-        out_specs=vmem,
+        out_shape=(
+            jax.ShapeDtypeStruct((half_rows, width), bf16),
+            jax.ShapeDtypeStruct(matrix.shape, f32),
+            jax.ShapeDtypeStruct((own_rows, here), f32),
+            jax.ShapeDtypeStruct((own_rows, matrix.shape[1]), f32),
+        ),
+        in_specs=[vmem] * len(resident) + [hbm] * len(streamed),
+        out_specs=(vmem, hbm, vmem, vmem),
         scratch_shapes=[
+            pltpu.VMEM((4, width, here), bf16),
+            pltpu.VMEM((here, width), bf16),
+            pltpu.VMEM(matrix.shape, f32),
+            pltpu.VMEM((matrix.shape[1], own_rows, matrix.shape[2]), f32),
+            pltpu.VMEM((own_rows, width + LANES), f32),
             pltpu.VMEM((width, hidden), bf16),
             pltpu.VMEM((width, hidden), bf16),
             pltpu.VMEM((hidden, width), bf16),
@@ -365,17 +437,17 @@
             pltpu.VMEM((members, half_rows, width), bf16),
             pltpu.VMEM((2, half_rows, half), f32),
             pltpu.VMEM((half_rows, half), f32),
-            pltpu.SemaphoreType.DMA((3,)),
+            pltpu.SemaphoreType.DMA((8 + 2 * CHUNKS,)),
             pltpu.SemaphoreType.DMA((8,)),
             pltpu.SemaphoreType.DMA((8,)),
             pltpu.SemaphoreType.DMA((2 * nx + span * nx,)),
             pltpu.SemaphoreType.DMA((2 * span * nx,)),
         ],
         compiler_params=pltpu.CompilerParams(
-            collective_id=0, has_side_effects=True, vmem_limit_bytes=48 * 1024 * 1024
+            collective_id=0, has_side_effects=True, vmem_limit_bytes=60 * 1024 * 1024
         ),
         name="feed",
-    )(tokens, part, routes, scores, gain, blend, block, gate, up, down)
+    )(*resident, *streamed)
 
 
 def local(
@@ -407,53 +479,39 @@
     blend_weight,
 ):
     own_rows = tokens.shape[0]
-    heads_here = forget_bias.shape[0]
-    head_size = head_gain.shape[1]
-    width_here = heads_here * head_size
-    normed = rms_norm(tokens, mixer_gain)
-
-    def project(weight):
-        return jnp.dot(normed, weight, preferred_element_type=jnp.float32)
-
-    query = project(query_weight).reshape(own_rows, heads_here, head_size)
-    key_rows = project(key_weight).reshape(own_rows, heads_here, head_size) * head_size ** (-0.5)
-    value_rows = project(value_weight).reshape(own_rows, heads_here, head_size)
-    outgate_rows = project(outgate_weight).reshape(own_rows, heads_here, head_size)
-    in_gate = project(ingate_weight)
-    forget_pre = project(forget_weight) + forget_bias
-    readout, matrix, norm_vec, new_max = memory_step(
-        query, key_rows, value_rows, in_gate, forget_pre, memory_matrix, memory_norm, memory_max
-    )
-    energy = jnp.sum(readout * readout, axis=(1, 2))
-    gated = (
-        (readout * head_gain * jax.nn.sigmoid(outgate_rows))
-        .reshape(own_rows, width_here)
-        .astype(jnp.bfloat16)
-    )
-    head_part = jnp.dot(gated, merge_weight, preferred_element_type=jnp.float32)
-    part = jnp.concatenate([head_part, jnp.broadcast_to(energy[:, None], (own_rows, LANES))], axis=1)
 
     def padded(rows):
         return jnp.pad(rows, ((0, PADDED - rows.shape[0]), (0, 0)))
 
     block = jnp.concatenate([padded(dense_left.T), padded(dense_right.T), padded(dense_down)], axis=0)
-    layer_out = feed(
-        lax.axis_size("ep"),
-        nx,
-        span,
-        width_here * lax.axis_size("tp"),
+    resident = (
         tokens,
-        part,
         routes,
         route_scores,
+        mixer_gain[None, :],
         feed_gain[None, :],
         blend_weight[None, :],
         block,
+        jnp.concatenate([ingate_weight, forget_weight], axis=1),
+        forget_bias[None, :],
+        head_gain,
+        memory_norm.reshape(own_rows, -1),
+        memory_max,
+    )
+    streamed = (
+        query_weight,
+        key_weight,
+        value_weight,
+        outgate_weight,
+        merge_weight,
+        memory_matrix,
         expert_gate,
         expert_up,
         expert_down,
     )
-    return (layer_out, matrix, norm_vec, new_max)
+    all_width = query_weight.shape[1] * lax.axis_size("tp")
+    layer_out, matrix, norm, new_max = feed(lax.axis_size("ep"), nx, span, all_width, resident, streamed)
+    return (layer_out, matrix, norm.reshape(memory_norm.shape), new_max)
 
 
 def build(mesh, nx, span):

time: 84.1 us -> 83.7 us (level)
  matrix products: 9.84 us -> 0 us
  local copies, waits for them, and re-layouts: 4.36 us -> 13.4 us
  Pallas kernels: 64.2 us -> 66.7 us
  other arithmetic: 4.51 us -> 2.45 us
    dot_general x8 -> x0, matrix products: 9.84 us -> none  [the longest x6 6.07 us: project(): return jnp.dot(normed, weight, preferred_element_type=jnp.float32)]
    unnamed x37 -> x7, local copies, waits for them, and re-layouts: 3.87 us -> 11.1 us
    reduce_sum x3 -> x0, other arithmetic: 2.66 us -> none  [the longest x1 1.43 us: memory_step(): denom = jnp.sum(query_rows * norm_vec, axis=-1)]
    pallas_call x1, Pallas kernels: 64.2 us -> 66.7 us  [feed(): pl.pallas_call(functools.partial(feed_kernel, nep, nx, span, all_width),...]
    add x1 -> x0, other arithmetic: 1.71 us -> none  [memory_step(): keep[..., None, None] * matrix]
    concatenate x1, other arithmetic: 0.02 us -> 1.73 us  [local(): jnp.concatenate([padded(dense_left.T), padded(dense_right.T), padded(dens...]
    reshape x3 -> x1, local copies, waits for them, and re-layouts: 0.05 us -> 1.33 us  [local(): return (layer_out, matrix, norm.reshape(memory_norm.shape), new_max)]
    concatenate x0 -> x1, local copies, waits for them, and re-layouts: none -> 0.92 us  [local(): jnp.concatenate([ingate_weight, forget_weight], axis=1)]
where the time goes in v2:
time: 83.7 us; the launch traced here: 83.2 us
  Pallas kernels  66.7 us (80%)
  local copies, waits for them, and re-layouts  13.4 us (16%)
  other arithmetic  2.45 us (3%)
    pallas_call x1, Pallas kernels, feed(): pl.pallas_call(functools.partial(feed_kernel, nep, nx, span, all_width),...  66.7 us
    unnamed x7, local copies, waits for them, and re-layouts  11.1 us
    concatenate x1, other arithmetic, local(): jnp.concatenate([padded(dense_left.T), padded(dense_right.T), padded(dens...  1.73 us

profile of v2, /device:TPU:40, one launch (start us, length us, event | category | flops | bytes accessed | tf_op | source)
XLA Modules:
  0.0 83.2 jit_solution(13993754530048609297)
XLA Ops:
  0.6 1.3 %copy.35.scores_ref = bf16[16,2]{1,0:T(8,128)(2,1)} copy(bf16[16,2]{0,1:T(2,128)(2,1)} %param.40) | data formatting | bytes 128 | tf_op args[16]
  2.0 0.7 pad_maximum_fusion
  2.7 1.3 %copy.37.max_ref = f32[16,2]{1,0:T(8,128)} copy(f32[16,2]{0,1:T(2,128)} %param.38) | data formatting | bytes 256 | tf_op args[14]
  4.0 1.4 %copy.34.routes_ref = s32[16,2]{1,0:T(8,128)} copy(s32[16,2]{0,1:T(2,128)} %param.39) | data formatting | bytes 256 | tf_op args[15]
  5.4 1.3 %copy.41 = f32[2,8,2,128]{3,1,2,0:T(8,128)} copy(f32[2,8,2,128]{3,2,1,0:T(2,128)} %bitcast.13) | data formatting | bytes 32768
  6.7 0.9 %copy.36.inforget_ref = bf16[1024,4]{1,0:T(8,128)(2,1)} copy(bf16[1024,4]{0,1:T(4,128)(2,1)S(1)} %pad_maximum_fusion) | data formatting | bytes 16384 | tf_op jit(solution)/shard_map/concatenate | solution.py:495
  7.6 1.7 %fusion.5.block_ref = bf16[144,1024]{1,0:T(8,128)(2,1)} fusion(bf16[44,1024]{1,0:T(8,128)(2,1)} %param.46, bf16[44,1024]{1,0:T(8,128)(2,1)} %bitcast.10, bf16[44,1024]{1,0:T(8,128)(2,1)} %bitcast.11), kind=kLoop, calls=%fused_computation.9 | loop fusion | flops 2064384 | bytes 565248 | tf_op jit(solution)/shard_map/concatenate | solution.py:486
  9.3 66.7 %feed.1 = (bf16[8,1024]{1,0:T(8,128)(2,1)}, f32[16,2,128,128]{3,2,1,0:T(8,128)}, f32[16,256]{1,0:T(8,128)}, f32[16,2]{1,0:T(8,128)}) custom-call(bf16[16,1024]{1,0:T(8,128)(2,1)} %tokens_ref.1, s32[16,2]{1,0:T(8,128)} %copy.34.routes_ref, bf16[16,2]{1,0:T(8,128)(2,1)} %copy.35.scores_ref, f32[1,1024]{1,0:T(1,128)} %bitcast.14, f32[1,1024]{1,0:T(1,128)} %bitcast.15, ...), custom_call_target="tpu_custom_call" | custom-call | tf_op jit(solution)/shard_map/feed/pallas_call | solution.py:403
  76.0 1.3 %copy.38 = f32[16,2]{0,1:T(2,128)} copy(f32[16,2]{1,0:T(8,128)} %get-tuple-element.19) | data formatting | bytes 256
  77.4 1.3 %reshape.15 = f32[16,2,128]{2,1,0:T(2,128)} reshape(f32[16,256]{1,0:T(8,128)} %get-tuple-element.10) | data formatting | bytes 32768 | tf_op jit(solution)/shard_map/reshape | solution.py:514
  78.7 1.3 %copy.44 = bf16[8,1024]{1,0:T(8,128)(2,1)} copy(bf16[8,1024]{1,0:T(8,128)(2,1)} %get-tuple-element.24) | data formatting | bytes 32768
  80.0 3.1 %copy.45 = f32[16,2,128,128]{3,2,1,0:T(8,128)} copy(f32[16,2,128,128]{3,2,1,0:T(8,128)} %get-tuple-element.25) | data formatting | bytes 4194304

commit v3 on v2

--- a/solution.py
+++ b/solution.py
@@ -48,8 +48,11 @@
     mixer_ref,
     gain_ref,
     blend_ref,
-    block_ref,
-    inforget_ref,
+    left_ref,
+    right_ref,
+    down_ref,
+    ingate_ref,
+    forget_ref,
     bias_ref,
     head_gain_ref,
     norm_ref,
@@ -64,12 +67,11 @@
     up_hbm,
     down_hbm,
     out_ref,
-    new_matrix_hbm,
+    matrix_v,
     new_norm_ref,
     new_max_ref,
     project_v,
     merge_v,
-    matrix_v,
     numer_v,
     part_ref,
     gate_v,
@@ -135,23 +137,31 @@
         moves.append((matrix_hbm.at[rows], matrix_v.at[rows]))
     moves += [(merge_hbm, merge_v), (gate_hbm.at[0], gate_v), (up_hbm.at[0], up_v), (down_hbm.at[0], down_v)]
     loads = [pltpu.make_async_copy(src, dst, local_sem.at[i]) for i, (src, dst) in enumerate(moves)]
-    stores = [
-        pltpu.make_async_copy(dst, new_matrix_hbm.at[pl.ds(c * chunk, chunk)], local_sem.at[len(loads) + c])
-        for c, (_, dst) in enumerate(moves[4 : 4 + CHUNKS])
-    ]
     for load in loads:
         load.start()
-    blocks[my_block] = block_ref[...]
+    spare = jnp.zeros((PADDED - left_ref.shape[0], width), jnp.bfloat16)
+    for i, ref in enumerate((left_ref, right_ref, down_ref)):
+        blocks[my_block, i * PADDED : (i + 1) * PADDED, :] = jnp.concatenate([ref[...], spare], axis=0)
     mine = pl.ds(pl.multiple_of(t * half, LANES), half)
 
     heads, head = head_gain_ref.shape
+    row_at = lax.broadcasted_iota(jnp.int32, (own_rows, own_rows), 0)
+    col_at = lax.broadcasted_iota(jnp.int32, (own_rows, own_rows), 1)
+    same = row_at == col_at
+
+    def upright(rows):
+        rows = rows.astype(jnp.float32)
+        return [
+            jnp.sum(jnp.where(same, rows[i : i + 1, :], 0.0), axis=1, keepdims=True) for i in range(rows.shape[0])
+        ]
+
     first = rms_norm(tokens_ref[...], mixer_ref[...])
-    gates = dot32(first, inforget_ref[...])
-    in_gate = gates[:, 0:heads]
-    log_forget = jax.nn.log_sigmoid(gates[:, heads : 2 * heads] + bias_ref[...])
-    old_max = max_ref[...]
+    in_gate = dot_nt(first, ingate_ref[...])
+    log_forget = jax.nn.log_sigmoid(dot_nt(first, forget_ref[...]) + bias_ref[...])
+    old_max = jnp.concatenate(upright(max_ref[...]), axis=1)
     new_max = jnp.maximum(log_forget + old_max, in_gate)
-    new_max_ref[...] = new_max
+    for h in range(heads):
+        new_max_ref[h : h + 1, :] = jnp.sum(jnp.where(same, new_max[:, h : h + 1], 0.0), axis=0, keepdims=True)
     keep = jnp.exp(log_forget + old_max - new_max)
     write = jnp.exp(in_gate - new_max)
     floor = jnp.exp(-new_max)
@@ -165,8 +175,8 @@
     columns = jnp.concatenate(queries + written, axis=0).T
     norms = []
     for h in range(heads):
-        norm = keep[:, h : h + 1] * norm_ref[:, h * head : (h + 1) * head] + written[h]
-        new_norm_ref[:, h * head : (h + 1) * head] = norm
+        norm = keep[:, h : h + 1] * norm_ref[:, h, :] + written[h]
+        new_norm_ref[:, h, :] = norm
         norms.append(norm)
     for b in range(own_rows):
         if b % chunk == 0:
@@ -177,8 +187,6 @@
             fresh = keep[b : b + 1, h : h + 1] * matrix_v[b, h] + columns[:, to : to + 1] * values[h][b : b + 1, :]
             matrix_v[b, h] = fresh
             numer_v[h, b : b + 1, :] = jnp.sum(columns[:, at : at + 1] * fresh, axis=0, keepdims=True)
-        if b % chunk == chunk - 1:
-            stores[b // chunk].start()
     energy = jnp.zeros((own_rows, 1), jnp.float32)
     gated = []
     for h in range(heads):
@@ -212,11 +220,9 @@
     normed = rms_norm(resid32, gain_ref[...])
     normed_v[...] = normed.astype(jnp.float32)
 
-    experts = lax.broadcasted_iota(jnp.int32, (own_rows, nep), 1)
-    picks = [(routes_ref[:, k : k + 1] == experts).astype(jnp.float32) for k in range(2)]
+    experts = lax.broadcasted_iota(jnp.int32, (own_rows, nep), 1).astype(jnp.float32)
+    picks = [(named == experts).astype(jnp.float32) for named in upright(routes_ref[...])]
     member = picks[0] + picks[1]
-    row_at = lax.broadcasted_iota(jnp.int32, (own_rows, own_rows), 0)
-    col_at = lax.broadcasted_iota(jnp.int32, (own_rows, own_rows), 1)
     earlier = (col_at < row_at).astype(jnp.float32)
     rank = dot32(earlier, member)
     chosen = [jnp.where(rank < 0.5, member, 0.0), jnp.where(rank < 0.5, 0.0, member)]
@@ -342,11 +348,10 @@
 
     dense_in[zi] = dense_out[zi]
 
-    scores = scores_ref[...].astype(jnp.float32)
-    top = jnp.max(scores, axis=-1, keepdims=True)
-    powers = jnp.exp(scores - top)
-    weights = powers / jnp.sum(powers, axis=-1, keepdims=True)
-    weight_of = weights[:, 0:1] * picks[0] + weights[:, 1:2] * picks[1]
+    scores = upright(scores_ref[...])
+    top = jnp.maximum(scores[0], scores[1])
+    powers = [jnp.exp(score - top) for score in scores]
+    weight_of = (powers[0] * picks[0] + powers[1] * picks[1]) / (powers[0] + powers[1])
     await_bytes(homebox.at[pl.ds(0, peers)], recv_sem.at[5])
     relay[...] = homebox[...].astype(jnp.float32).reshape(relay.shape)
     routed = []
@@ -372,8 +377,6 @@
     out_ref[:, mine] = (resid_v[home, mine] + swap_out[t]).astype(jnp.bfloat16)
     out_ref[:, theirs] = (resid_v[home, theirs] + swap_in[...]).astype(jnp.bfloat16)
 
-    for store in stores:
-        store.wait()
     await_bytes(act_bytes, send_sem.at[2])
     box_swap.wait_send()
     half_swap.wait_send()
@@ -403,17 +406,16 @@
     return pl.pallas_call(
         functools.partial(feed_kernel, nep, nx, span, all_width),
         out_shape=(
-            jax.ShapeDtypeStruct((half_rows, width), bf16),
-            jax.ShapeDtypeStruct(matrix.shape, f32),
-            jax.ShapeDtypeStruct((own_rows, here), f32),
-            jax.ShapeDtypeStruct((own_rows, matrix.shape[1]), f32),
+            pltpu.VMEM((half_rows, width), bf16),
+            pltpu.VMEM(matrix.shape, f32),
+            pltpu.VMEM((own_rows, *matrix.shape[1:3]), f32),
+            pltpu.VMEM((matrix.shape[1], own_rows), f32),
         ),
         in_specs=[vmem] * len(resident) + [hbm] * len(streamed),
-        out_specs=(vmem, hbm, vmem, vmem),
+        out_specs=(vmem, vmem, vmem, vmem),
         scratch_shapes=[
             pltpu.VMEM((4, width, here), bf16),
             pltpu.VMEM((here, width), bf16),
-            pltpu.VMEM(matrix.shape, f32),
             pltpu.VMEM((matrix.shape[1], own_rows, matrix.shape[2]), f32),
             pltpu.VMEM((own_rows, width + LANES), f32),
             pltpu.VMEM((width, hidden), bf16),
@@ -437,17 +439,42 @@
             pltpu.VMEM((members, half_rows, width), bf16),
             pltpu.VMEM((2, half_rows, half), f32),
             pltpu.VMEM((half_rows, half), f32),
-            pltpu.SemaphoreType.DMA((8 + 2 * CHUNKS,)),
+            pltpu.SemaphoreType.DMA((8 + CHUNKS,)),
             pltpu.SemaphoreType.DMA((8,)),
             pltpu.SemaphoreType.DMA((8,)),
             pltpu.SemaphoreType.DMA((2 * nx + span * nx,)),
             pltpu.SemaphoreType.DMA((2 * span * nx,)),
         ],
         compiler_params=pltpu.CompilerParams(
-            collective_id=0, has_side_effects=True, vmem_limit_bytes=60 * 1024 * 1024
+            collective_id=0, has_side_effects=True, vmem_limit_bytes=61 * 1024 * 1024
         ),
         name="feed",
     )(*resident, *streamed)
+
+
+def finish_kernel(layer_in, matrix_in, norm_in, max_in, layer_out, matrix_out, norm_out, max_out, sem):
+    copies = [
+        pltpu.make_async_copy(src, dst, sem.at[i])
+        for i, (src, dst) in enumerate(
+            ((matrix_in, matrix_out), (layer_in, layer_out), (norm_in, norm_out), (max_in, max_out))
+        )
+    ]
+    for copy in copies:
+        copy.start()
+    for copy in copies:
+        copy.wait()
+
+
+def finish(arrays):
+    return pl.pallas_call(
+        finish_kernel,
+        out_shape=tuple(jax.ShapeDtypeStruct(a.shape, a.dtype) for a in arrays),
+        in_specs=[pl.BlockSpec(memory_space=pltpu.VMEM)] * len(arrays),
+        out_specs=tuple([pl.BlockSpec(memory_space=pltpu.HBM)] * len(arrays)),
+        scratch_shapes=[pltpu.SemaphoreType.DMA((len(arrays),))],
+        compiler_params=pltpu.CompilerParams(vmem_limit_bytes=16 * 1024 * 1024),
+        name="finish",
+    )(*arrays)
 
 
 def local(
@@ -478,25 +505,22 @@
     dense_down,
     blend_weight,
 ):
-    own_rows = tokens.shape[0]
-
-    def padded(rows):
-        return jnp.pad(rows, ((0, PADDED - rows.shape[0]), (0, 0)))
-
-    block = jnp.concatenate([padded(dense_left.T), padded(dense_right.T), padded(dense_down)], axis=0)
     resident = (
         tokens,
-        routes,
-        route_scores,
+        routes.T,
+        route_scores.T,
         mixer_gain[None, :],
         feed_gain[None, :],
         blend_weight[None, :],
-        block,
-        jnp.concatenate([ingate_weight, forget_weight], axis=1),
+        dense_left.T,
+        dense_right.T,
+        dense_down,
+        ingate_weight.T,
+        forget_weight.T,
         forget_bias[None, :],
         head_gain,
-        memory_norm.reshape(own_rows, -1),
-        memory_max,
+        memory_norm,
+        memory_max.T,
     )
     streamed = (
         query_weight,
@@ -510,8 +534,9 @@
         expert_down,
     )
     all_width = query_weight.shape[1] * lax.axis_size("tp")
-    layer_out, matrix, norm, new_max = feed(lax.axis_size("ep"), nx, span, all_width, resident, streamed)
-    return (layer_out, matrix, norm.reshape(memory_norm.shape), new_max)
+    results = feed(lax.axis_size("ep"), nx, span, all_width, resident, streamed)
+    layer_out, matrix, norm, new_max = finish(results)
+    return (layer_out, matrix, norm, new_max.T)
 
 
 def build(mesh, nx, span):

time: 83.7 us -> 68.6 us (0.82)
  local copies, waits for them, and re-layouts: 13.4 us -> 0 us
  other arithmetic: 2.45 us -> 0 us
  Pallas kernels: 66.7 us -> 67.8 us
    unnamed x7 -> x0, local copies, waits for them, and re-layouts: 11.1 us -> none
    concatenate x2 -> x0, other arithmetic: 2.45 us -> none  [the longest x1 1.73 us: local(): jnp.concatenate([padded(dense_left.T), padded(dense_right.T), padded(dens...]
    pallas_call x0 -> x1, Pallas kernels: none -> 1.36 us  [finish(): pl.pallas_call(finish_kernel, out_shape=tuple((jax.ShapeDtypeStruct(a.sha...]
    reshape x1 -> x0, local copies, waits for them, and re-layouts: 1.33 us -> none  [local(): return (layer_out, matrix, norm.reshape(memory_norm.shape), new_max)]
    concatenate x1 -> x0, local copies, waits for them, and re-layouts: 0.92 us -> none  [local(): jnp.concatenate([ingate_weight, forget_weight], axis=1)]
where the time goes in v3:
time: 68.6 us; the launch traced here: 68.5 us
  Pallas kernels  67.8 us (99%)
    pallas_call x1, Pallas kernels, feed(): pl.pallas_call(functools.partial(feed_kernel, nep, nx, span, all_width),...  66.5 us

profile of v3, /device:TPU:40, one launch (start us, length us, event | category | flops | bytes accessed | tf_op | source)
XLA Modules:
  0.0 68.5 jit_solution(2905150512600909124)
XLA Ops:
  0.6 66.5 %feed.1 = (bf16[8,1024]{1,0:T(8,128)(2,1)S(1)}, f32[16,2,128,128]{3,2,1,0:T(8,128)S(1)}, f32[16,2,128]{2,1,0:T(2,128)S(1)}, f32[2,16]{1,0:T(2,128)S(1)}) custom-call(bf16[16,1024]{1,0:T(8,128)(2,1)} %tokens_ref.1, s32[2,16]{1,0:T(2,128)} %bitcast.19, bf16[2,16]{1,0:T(2,128)(2,1)} %bitcast.21, f32[1,1024]{1,0:T(1,128)} %bitcast.14, f32[1,1024]{1,0:T(1,128)} %bitcast.15, ...), custom_call_target="tpu_custom_call" | custom-call | tf_op jit(solution)/shard_map/feed/pallas_call | solution.py:406
  67.1 1.4 %finish.1 = (bf16[8,1024]{1,0:T(8,128)(2,1)}, f32[16,2,128,128]{3,2,1,0:T(8,128)}, f32[16,2,128]{2,1,0:T(2,128)}, f32[2,16]{1,0:T(2,128)}) custom-call(bf16[8,1024]{1,0:T(8,128)(2,1)S(1)} %get-tuple-element.12.layer_in, f32[16,2,128,128]{3,2,1,0:T(8,128)S(1)} %get-tuple-element.13.matrix_in, f32[16,2,128]{2,1,0:T(2,128)S(1)} %get-tuple-element.14.norm_in, ...), custom_call_target="tpu_custom_call" | custom-call | tf_op jit(solution)/shard_map/finish/pallas_call | solution.py:469
